TPU v7x, 512 devices: a whole 4x4x16 slice. The times are simulated.
512 devices in a mesh: gr: 2 (over z_hi), sp: 32 (over z_lo, y), tp: 8 (over x, core).
Axes of the slice: x: 4, y: 4, z: 16 (z_hi: 2, z_lo: 8; z = z_hi * 8 + z_lo), core: 2. Of those that a mesh axis runs over, the one named last changes fastest.
Arguments:
- tokens: bfloat16 [8, 8192, 2048], P('gr', 'sp'), parts along dimension 0, may hold values from -6 to 6
- new_rows: bfloat16 [8, 2048], P('gr'), parts along dimension 0, may hold values from -6 to 6
- new_query: bfloat16 [8, 1024], P('gr', 'tp'), parts along dimension 0, may hold values from -6 to 6
- norm_gain: bfloat16 [2048], replicated, may hold values from 0.099609375 to 1.8984375
- key_weight: bfloat16 [2048, 1024], P('sp', 'tp'), may hold values from -0.125 to 0.125
- value_weight: bfloat16 [2048, 2048], P('sp', 'tp'), may hold values from -0.125 to 0.125
- input_weight: bfloat16 [2048, 16], replicated, may hold values from -0.125 to 0.125
- forget_weight: bfloat16 [2048, 16], replicated, may hold values from -0.125 to 0.125
- forget_bias: float32 [16], P('tp'), may hold values from 3 to 12
- gate_offsets: float32 [8, 8192, 2, 16], P('gr', 'sp', None, 'tp'), parts along dimension 0, may hold values from -6 to 250, as said below
Outputs:
- cache_keys: bfloat16 [64, 1024, 1024], P(('gr', 'sp'), None, 'tp'), parts along dimension 0
- cache_values: bfloat16 [64, 1024, 2048], P(('gr', 'sp'), None, 'tp'), parts along dimension 0
- cache_weights: float32 [64, 16, 1024], P(('gr', 'sp'), 'tp'), parts along dimension 0
- first_read: bfloat16 [8, 2048], P('gr', 'tp'), parts along dimension 0
There are 2 independent parts, one for each index of `gr`. A program takes and returns all parts, laid end to end along the dimension named above; an argument that names none is the same for every part. Nothing has to cross between parts.
Inputs may be any that keep to these rules, and one draw needn't show every extreme that they name: `gate_offsets`: entry 1 along the third dimension is never positive.
All inputs are finite; a program needn't handle non-finite values.
Results may differ from a plain program's by a relative error of at most 0.012.
The roundings to bfloat16 on the way count: a program that leaves them out, or rounds other values in their place, can miss the bound.
Values may be sent and summed in bfloat16 or wider, within the bound.
A program may use at most 64 MiB of HBM per device.

v0:
```python
import jax
import jax.numpy as jnp
from jax import lax
from jax.sharding import Mesh
from jax.sharding import PartitionSpec as P

SP = ("sp_0", "sp_1")
GR_SP = ("gr", "sp_0", "sp_1")


EPSILON = 1e-06


def in_one_piece(arrays, axis, dim, along):
    widths = [a.shape[along] for a in arrays]
    both = jnp.concatenate(arrays, axis=along)
    result = lax.all_gather(both, axis, axis=dim, tiled=True)
    return tuple(jnp.split(result, [sum(widths[:k]) for k in range(1, len(widths))], axis=along))


def side_by_side(arrays, axis, split_dim, concat_dim, along):
    ends, at = ([], 0)
    for a in arrays[:-1]:
        at += a.shape[along]
        ends.append(at)
    both = jnp.concatenate(arrays, axis=along)
    return tuple(
        jnp.split(
            lax.all_to_all(both, axis, split_axis=split_dim, concat_axis=concat_dim, tiled=True),
            ends,
            axis=along,
        )
    )


def sent_to_all(x, axis):
    devices = lax.axis_size(axis)
    return lax.all_to_all(jnp.broadcast_to(x[None], (devices, *x.shape)), axis, 0, 0, tiled=True)


def combined_pairwise(pieces, combine):
    while len(jax.tree.leaves(pieces)[0]) > 1:
        pieces = jax.vmap(combine)(*(pieces[side::2] for side in (0, 1)))
    return pieces[0]


def entering(x, axis, combine, identity):
    devices, index = (lax.axis_size(axis), lax.axis_index(axis))
    passed = jnp.arange(devices) > index

    def kept(part, zero, own):
        part = jnp.where(
            passed.reshape(-1, *(1 for _ in own.shape)), part, jnp.asarray(zero, own.dtype)
        )
        return part[::-1]

    pieces = sent_to_all(x, axis)
    return combined_pairwise(kept(pieces, identity, x), combine)


def over_axes(x, axes):
    for axis in axes:
        x = lax.pmax(x, axis)
    return x


def taken_together(x, axis):
    return sent_to_all(x, axis).sum(axis=0)


def packed_total(arrays, axis):
    ends = [0]
    for a in arrays:
        ends.append(ends[-1] + a.size)
    subtotal = taken_together(jnp.concatenate([a.ravel() for a in arrays]), axis)
    return tuple((subtotal[b:e].reshape(a.shape) for a, b, e in zip(arrays, ends, ends[1:])))


def normed_rows(source, norm_gain):
    widened = source.astype(jnp.float32)
    inverse_rms = lax.rsqrt(jnp.mean(widened * widened, axis=-1, keepdims=True) + EPSILON)
    return (widened * inverse_rms * norm_gain.astype(jnp.float32)).astype(jnp.bfloat16)


def suffix_sums(log_forget):
    flipped = jnp.cumsum(jnp.flip(log_forget, 1), axis=1)
    return jnp.flip(flipped, 1) - log_forget


def add_totals(earlier, following):
    return earlier + following


def partial_read(query_heads, key_heads, value_heads, log_weight, peak_log):
    scores = jnp.einsum("nhd,nshd->nsh", query_heads, key_heads, preferred_element_type=jnp.float32)
    weighted_terms = jnp.exp(log_weight - peak_log[:, None, :]) * scores
    rounded = weighted_terms.astype(jnp.bfloat16)
    numerator = jnp.einsum(
        "nsh,nshd->nhd", rounded, value_heads, preferred_element_type=jnp.float32
    )
    return (numerator, jnp.sum(weighted_terms, axis=1))


def finish_read(numerator, denominator, peak_log, query_heads, key_new, value_new, gate_new):
    peak_new = jnp.maximum(peak_log, gate_new)
    old_part = jnp.exp(peak_log - peak_new)
    own_score = jnp.einsum("nhd,nhd->nh", query_heads, key_new, preferred_element_type=jnp.float32)
    new_part = jnp.exp(gate_new - peak_new) * own_score
    total_value = old_part[..., None] * numerator + new_part[..., None] * value_new.astype(
        jnp.float32
    )
    total_weight = old_part * denominator + new_part
    return total_value / jnp.maximum(jnp.abs(total_weight), 1.0)[..., None]


def per_device(
    tokens,
    new_rows,
    new_query,
    norm_gain,
    key_weight,
    value_weight,
    input_weight,
    forget_weight,
    forget_bias,
    gate_offsets,
):
    seq_count, positions, model_width = tokens.shape
    heads_here = forget_bias.shape[0]
    key_size = key_weight.shape[1] // heads_here
    value_size = value_weight.shape[1] // heads_here
    group_size = lax.axis_size(SP)
    pieces = group_size // seq_count
    sub_rows = positions // pieces
    prompt_rows = seq_count * positions
    normed_all = jnp.concatenate(
        [
            normed_rows(tokens, norm_gain).reshape(prompt_rows, model_width),
            normed_rows(new_rows, norm_gain),
        ],
        axis=0,
    )
    parts = in_one_piece((key_weight, value_weight), SP, 0, 1)
    key_sum = jnp.dot(normed_all, parts[0], preferred_element_type=jnp.float32)
    value_sum = jnp.dot(normed_all, parts[1], preferred_element_type=jnp.float32)
    keys_all = (key_sum * key_size ** (-0.5)).astype(jnp.bfloat16)
    values_all = value_sum.astype(jnp.bfloat16)
    head_start = lax.axis_index("tp") * heads_here
    input_all = lax.dynamic_slice_in_dim(
        jnp.dot(normed_all, input_weight, preferred_element_type=jnp.float32),
        head_start,
        heads_here,
        1,
    )
    forget_all = lax.dynamic_slice_in_dim(
        jnp.dot(normed_all, forget_weight, preferred_element_type=jnp.float32),
        head_start,
        heads_here,
        1,
    )
    key_rows = keys_all[:prompt_rows].reshape(seq_count, positions, heads_here * key_size)
    value_rows = values_all[:prompt_rows].reshape(seq_count, positions, heads_here * value_size)
    input_gate = (
        input_all[:prompt_rows].reshape(seq_count, positions, heads_here) + gate_offsets[:, :, 0, :]
    )
    log_forget = (
        jax.nn.log_sigmoid(
            forget_all[:prompt_rows].reshape(seq_count, positions, heads_here) + forget_bias
        )
        + gate_offsets[:, :, 1, :]
    )
    key_new = keys_all[prompt_rows:].reshape(seq_count, heads_here, key_size)
    value_new = values_all[prompt_rows:].reshape(seq_count, heads_here, value_size)
    gate_new = input_all[prompt_rows:]
    query_all = new_query.reshape(seq_count, heads_here, key_size)
    cache_keys, cache_values = side_by_side(
        (
            key_rows.reshape(seq_count * pieces, sub_rows, heads_here * key_size),
            value_rows.reshape(seq_count * pieces, sub_rows, heads_here * value_size),
        ),
        SP,
        0,
        1,
        2,
    )
    totals = jnp.sum(log_forget, axis=1)
    tail_sum = entering(totals, SP, add_totals, jnp.zeros_like(totals))
    log_weight = input_gate + suffix_sums(log_forget) + tail_sum[:, None, :]
    peak_all = over_axes(jnp.max(log_weight, axis=1), SP)
    numerator, denominator = partial_read(
        query_all,
        key_rows.reshape(seq_count, positions, heads_here, key_size),
        value_rows.reshape(seq_count, positions, heads_here, value_size),
        log_weight,
        peak_all,
    )
    numerator, denominator = packed_total((numerator, denominator), SP)
    cache_weight = lax.all_to_all(
        log_weight.reshape(seq_count * pieces, sub_rows, heads_here),
        SP,
        split_axis=0,
        concat_axis=1,
        tiled=True,
    )
    read_out = finish_read(
        numerator, denominator, peak_all, query_all, key_new, value_new, gate_new
    )
    return (
        cache_keys,
        cache_values,
        jnp.transpose(cache_weight, (0, 2, 1)),
        read_out.reshape(seq_count, heads_here * value_size).astype(jnp.bfloat16),
    )


def solution(mesh):
    finer = Mesh(
        mesh.devices.reshape(mesh.shape["gr"], 8, 4, mesh.shape["tp"]), ("gr", "sp_0", "sp_1", "tp")
    )
    in_specs = (
        P("gr", SP, None),
        P("gr", None),
        P("gr", "tp"),
        P(),
        P(SP, "tp"),
        P(SP, "tp"),
        P(),
        P(),
        P("tp"),
        P("gr", SP, None, "tp"),
    )
    out_specs = (P(GR_SP, None, "tp"), P(GR_SP, None, "tp"), P(GR_SP, "tp", None), P("gr", "tp"))
    return jax.shard_map(
        per_device, mesh=finer, in_specs=in_specs, out_specs=out_specs, check_vma=False
    )
```

profile of v0, /device:TPU:2, one launch (start us, length us, event | category | flops | bytes accessed | tf_op | source)
XLA Modules:
  0.0 313.1 jit_solution(10832528095023185210)
XLA Ops:
  7.2 1.4 pad_maximum_fusion.2
  8.7 1.0 fusion.10
  9.7 3.3 %fusion = f32[4,256]{1,0:T(4,128)S(1)} fusion(bf16[4,256,2048]{2,1,0:T(8,128)(2,1)} %param.10), kind=kLoop, calls=%fused_computation.2 | loop fusion | flops 6290432 | bytes 4198400 | tf_op jit(solution)/shard_map/reduce_sum | solution.py:81
  13.1 3.0 fusion.2
  16.1 3.6 %fusion.26 = f32[1028,16]{0,1:T(8,128)S(1)} fusion(bf16[2048,16]{0,1:T(8,128)(2,1)S(1)} %copy-done, bf16[4,2048]{1,0:T(4,128)(2,1)S(1)} %fusion.12, bf16[1024,2048]{1,0:T(8,128)(2,1)} %bitcast.67), kind=kOutput, calls=%fused_computation.62 | convolution fusion | flops 75792384 | bytes 4342016 | tf_op jit(solution)/shard_map/dot_general | solution.py:150
  19.8 1.3 fusion.25
  21.4 0.6 broadcast_in_dim.17
  22.0 15.5 %all-to-all-start.1 = ((f32[32,4,2]{1,2,0:T(2,128)}), f32[32,4,2]{1,2,0:T(2,128)S(1)}, u32[]{:S(2)}, u32[]{:S(2)}) async-start(f32[32,4,2]{1,2,0:T(2,128)} %broadcast_in_dim.17), calls=%async_computation.1 | async-start | bytes 65536 | tf_op jit(solution)/shard_map/all_to_all | solution.py:38
  37.6 0.2 rev.8
  37.8 2.4 reduce-window.6
  40.7 0.2 rev.9
  40.9 9.4 %all-to-all-done.1 = f32[32,4,2]{1,2,0:T(2,128)S(1)} async-done(((f32[32,4,2]{1,2,0:T(2,128)}), f32[32,4,2]{1,2,0:T(2,128)S(1)}, u32[]{:S(2)}, u32[]{:S(2)}) %all-to-all-start.1) | async-done | bytes 1056 | tf_op jit(solution)/shard_map/all_to_all | solution.py:38
  50.8 25.9 %pmax.14 = f32[4,2]{0,1:T(2,128)S(1)} all-reduce(f32[4,2]{0,1:T(2,128)S(1)} %copy.98), channel_id=1, replica_groups=mesh['gr'=2,'sp_0'=8,'sp_1'=4,'tp'=8] {'sp_0'}, use_global_device_ids=true, to_apply=%region_6.7 | all-reduce | flops 8 | bytes 64 | tf_op jit(solution)/shard_map/pmax | solution.py:63
  76.9 9.0 %pmax.15 = f32[4,2]{0,1:T(2,128)S(1)} all-reduce(f32[4,2]{0,1:T(2,128)S(1)} %pmax.14), channel_id=1, replica_groups=mesh['gr'=2,'sp_0'=8,'sp_1'=4,'tp'=8] {'sp_1'}, use_global_device_ids=true, to_apply=%region_7.8 | all-reduce | flops 8 | bytes 64 | tf_op jit(solution)/shard_map/pmax | solution.py:63
  86.1 0.6 copy.96
  86.7 3.9 %all-to-all-start.2 = ((f32[32,32,2]{1,2,0:T(2,128)}), f32[32,32,2]{1,2,0:T(2,128)S(1)}, u32[]{:S(2)}, u32[]{:S(2)}) async-start(f32[32,32,2]{1,2,0:T(2,128)} %copy.96), calls=%async_computation.2 | async-start | bytes 65536 | tf_op jit(solution)/shard_map/all_to_all | solution.py:198
  90.6 147.3 %all-gather.2.cloned.1.call-done = bf16[2048,384]{1,0:T(8,128)(2,1)} async-done(((bf16[64,384]{1,0:T(8,128)(2,1)}), bf16[2048,384]{1,0:T(8,128)(2,1)}) %all-gather.2.cloned.1.call-update) | async-done | bytes 1572880 | tf_op jit(solution)/shard_map/all_gather | solution.py:17
  237.9 3.7 %fusion.3 = bf16[1028,128]{1,0:T(8,128)(2,1)S(1)} fusion(bf16[2048,384]{1,0:T(8,128)(2,1)} %all-gather.2.cloned.1.call-done, bf16[4,2048]{1,0:T(4,128)(2,1)S(1)} %fusion.12, bf16[1024,2048]{1,0:T(8,128)(2,1)} %bitcast.68), kind=kOutput, calls=%fused_computation.8 | convolution fusion | flops 547652608 | bytes 4998144 | tf_op jit(solution)/shard_map/dot_general | solution.py:144
  241.6 0.3 copy-done.9
  242.0 1.4 convolution_convert_fusion
  243.5 0.2 reshape.122
  243.8 0.2 fusion.6
  244.5 0.7 broadcast_in_dim.19
  245.2 11.7 %all-to-all-start.3 = ((f32[32,1,1032]{2,1,0:T(1,128)}), f32[32,1,1032]{2,1,0:T(1,128)S(1)}, u32[]{:S(2)}, u32[]{:S(2)}) async-start(f32[32,1,1032]{2,1,0:T(1,128)} %broadcast_in_dim.19), calls=%async_computation.3 | async-start | bytes 294912 | tf_op jit(solution)/shard_map/all_to_all | solution.py:38
  256.9 1.0 pad_maximum_fusion.1
  257.9 18.0 %all-to-all-done.3 = f32[32,1,1032]{2,1,0:T(1,128)S(1)} async-done(((f32[32,1,1032]{2,1,0:T(1,128)}), f32[32,1,1032]{2,1,0:T(1,128)S(1)}, u32[]{:S(2)}, u32[]{:S(2)}) %all-to-all-start.3) | async-done | bytes 132128 | tf_op jit(solution)/shard_map/all_to_all | solution.py:38
  275.9 3.9 %all-to-all-start = ((bf16[32,32,384]{2,1,0:T(8,128)(2,1)}), bf16[32,32,384]{2,1,0:T(8,128)(2,1)S(1)}, u32[]{:S(2)}, u32[]{:S(2)}) async-start(bf16[32,32,384]{2,1,0:T(8,128)(2,1)} %pad_maximum_fusion.1), calls=%async_computation | async-start | bytes 1572864 | tf_op jit(solution)/shard_map/all_to_all | solution.py:29
  279.9 0.7 all_to_all.29
  281.8 0.6 fusion.20
  282.4 22.4 %all-to-all-done = bf16[32,32,384]{2,1,0:T(8,128)(2,1)S(1)} async-done(((bf16[32,32,384]{2,1,0:T(8,128)(2,1)}), bf16[32,32,384]{2,1,0:T(8,128)(2,1)S(1)}, u32[]{:S(2)}, u32[]{:S(2)}) %all-to-all-start) | async-done | bytes 786464 | tf_op jit(solution)/shard_map/all_to_all | solution.py:29
  304.7 0.7 split.18
  305.5 0.8 split.19
  (81 shorter events, 3.6 us)
Async XLA Ops:
  7.2 8.9 %copy-start = (bf16[2048,16]{0,1:T(8,128)(2,1)S(1)}, bf16[2048,16]{0,1:T(8,128)(2,1)}, u32[]{:S(2)}) copy-start(bf16[2048,16]{0,1:T(8,128)(2,1)} %param.16) | copy-start | bytes 196612
  7.2 5.8 %copy-start.6 = (bf16[2048]{0:T(1024)(128)(2,1)S(1)}, bf16[2048]{0:T(1024)(128)(2,1)}, u32[]{:S(2)}) copy-start(bf16[2048]{0:T(1024)(128)(2,1)} %param.13) | copy-start | bytes 12292
  7.2 230.7 %all-gather.2.cloned.1.call-start = ((), (), s32[]{:S(2)}) async-start(), calls=%async_computation.4 | async-start | bytes 1622016 | tf_op jit(solution)/shard_map/all_gather | solution.py:17
  8.7 4.4 %copy-start.1 = (bf16[4,256,2048]{2,1,0:T(8,128)(2,1)S(1)}, bf16[4,256,2048]{2,1,0:T(8,128)(2,1)}, u32[]{:S(2)}) copy-start(bf16[4,256,2048]{2,1,0:T(8,128)(2,1)} %param.10) | copy-start | bytes 12582916
  13.0 3.0 copy-start.4
  16.1 3.6 %copy-start.2 = (bf16[4,256,2048]{2,1,0:T(8,128)(2,1)S(1)}, bf16[4,256,2048]{2,1,0:T(8,128)(2,1)}, u32[]{:S(2)}) copy-start(bf16[4,256,2048]{2,1,0:T(8,128)(2,1)} %fusion.2) | copy-start | bytes 12582916
  16.1 3.6 %copy-start.10 = (bf16[2048,16]{0,1:T(8,128)(2,1)S(1)}, bf16[2048,16]{0,1:T(8,128)(2,1)}, u32[]{:S(2)}) copy-start(bf16[2048,16]{0,1:T(8,128)(2,1)} %param.17) | copy-start | bytes 196612
  19.7 1.4 copy-start.5
  19.7 1.4 copy-start.8
  19.7 57.0 %copy-start.7 = (bf16[4,128]{1,0:T(4,128)(2,1)S(1)}, bf16[4,128]{1,0:T(4,128)(2,1)}, u32[]{:S(2)}) copy-start(bf16[4,128]{1,0:T(4,128)(2,1)} %param.12) | copy-start | bytes 3076
  22.0 28.3 %all-to-all-start.1 = ((f32[32,4,2]{1,2,0:T(2,128)}), f32[32,4,2]{1,2,0:T(2,128)S(1)}, u32[]{:S(2)}, u32[]{:S(2)}) async-start(f32[32,4,2]{1,2,0:T(2,128)} %broadcast_in_dim.17), calls=%async_computation.1 | async-start | bytes 65536 | tf_op jit(solution)/shard_map/all_to_all | solution.py:38
  86.7 157.8 %all-to-all-start.2 = ((f32[32,32,2]{1,2,0:T(2,128)}), f32[32,32,2]{1,2,0:T(2,128)S(1)}, u32[]{:S(2)}, u32[]{:S(2)}) async-start(f32[32,32,2]{1,2,0:T(2,128)} %copy.96), calls=%async_computation.2 | async-start | bytes 65536 | tf_op jit(solution)/shard_map/all_to_all | solution.py:198
  237.9 3.8 %copy-start.3 = (bf16[4,256,2048]{2,1,0:T(8,128)(2,1)S(1)}, bf16[4,256,2048]{2,1,0:T(8,128)(2,1)}, u32[]{:S(2)}) copy-start(bf16[4,256,2048]{2,1,0:T(8,128)(2,1)} %fusion.2) | copy-start | bytes 12582916
  237.9 4.1 %copy-start.9 = (bf16[2048,384]{1,0:T(8,128)(2,1)S(1)}, bf16[2048,384]{1,0:T(8,128)(2,1)}, u32[]{:S(2)}) copy-start(bf16[2048,384]{1,0:T(8,128)(2,1)} %all-gather.2.cloned.1.call-done) | copy-start | bytes 4718596
  245.2 30.7 %all-to-all-start.3 = ((f32[32,1,1032]{2,1,0:T(1,128)}), f32[32,1,1032]{2,1,0:T(1,128)S(1)}, u32[]{:S(2)}, u32[]{:S(2)}) async-start(f32[32,1,1032]{2,1,0:T(1,128)} %broadcast_in_dim.19), calls=%async_computation.3 | async-start | bytes 294912 | tf_op jit(solution)/shard_map/all_to_all | solution.py:38
  275.9 28.8 %all-to-all-start = ((bf16[32,32,384]{2,1,0:T(8,128)(2,1)}), bf16[32,32,384]{2,1,0:T(8,128)(2,1)S(1)}, u32[]{:S(2)}, u32[]{:S(2)}) async-start(bf16[32,32,384]{2,1,0:T(8,128)(2,1)} %pad_maximum_fusion.1), calls=%async_computation | async-start | bytes 1572864 | tf_op jit(solution)/shard_map/all_to_all | solution.py:29
Sparse Core Ops, SparseCore 0:
  10.7 227.1 all-gather.1
where the time goes:
time: 314 us; the launch traced here: 313 us
  waiting for transfers between devices  197 us (63%)
  starting transfers between devices  35 us (11%)
  blocking collectives  35 us (11%)
  between operations  14.4 us (5%)
  other arithmetic  13.9 us (4%)
  matrix products  10.4 us (3%)
  local copies, waits for them, and re-layouts  7.45 us (2%)
    all_gather x1, waiting for transfers between devices, in_one_piece(): result = lax.all_gather(both, axis, axis=dim, tiled=True)  147 us
    pmax x2, blocking collectives, over_axes(): x = lax.pmax(x, axis)  35 us
    all_to_all x2, waiting for transfers between devices, sent_to_all(): lax.all_to_all(jnp.broadcast_to(x[None], (devices, *x.shape)), axis, 0, 0...  27.4 us
    all_to_all x2, starting transfers between devices, sent_to_all(): lax.all_to_all(jnp.broadcast_to(x[None], (devices, *x.shape)), axis, 0, 0...  27.2 us
    all_to_all x1, waiting for transfers between devices, side_by_side(): lax.all_to_all(both, axis, split_axis=split_dim, concat_axis=concat_dim,...  22.4 us
  transfers between devices with their start and end apart: 5, of which 4 were waited for; matrix products, arithmetic and copies ran while one was open for 9% of the time, Pallas kernels for 0%

commit v1 on v0

v1 whole, which is shorter than its diff:
```python
import jax
import jax.numpy as jnp
from jax import lax
from jax.experimental import pallas as pl
from jax.experimental.pallas import tpu as pltpu
from jax.sharding import PartitionSpec as P

EPSILON = 1e-06
MESH = pl.DeviceIdType.MESH
F32 = jnp.float32
BF16 = jnp.bfloat16
NT = (((1,), (1,)), ((), ()))

D = 2048
ROWS = 1024
GROUP = 256
BLOCK = 32
CHUNK = 64


def iota(shape, dim):
    return lax.broadcasted_iota(jnp.int32, shape, dim)


def xor2(a, b):
    return 2 * ((a // 2 + b // 2) % 2) + (a % 2 + b % 2) % 2


def norm_chunk(read, write, gain_ref, rows):
    total = jnp.zeros((rows, 128), F32)
    for c in range(D // 128):
        v = read(c).astype(F32)
        total = total + v * v
    inverse = lax.rsqrt(jnp.sum(total, axis=-1, keepdims=True) * (1.0 / D) + EPSILON)
    for c in range(D // 128):
        v = read(c).astype(F32)
        write(c, (v * inverse * gain_ref[:, c * 128 : (c + 1) * 128].astype(F32)).astype(BF16))


def norm_group(src, start, dst, gain_ref):
    def body(u, carry):
        at = pl.multiple_of(start + u * CHUNK, CHUNK)
        to = pl.multiple_of(u * CHUNK, CHUNK)

        def read(c):
            return src[pl.ds(at, CHUNK), c * 128 : (c + 1) * 128]

        def write(c, v):
            dst[pl.ds(to, CHUNK), c * 128 : (c + 1) * 128] = v

        norm_chunk(read, write, gain_ref, CHUNK)
        return carry

    lax.fori_loop(0, GROUP // CHUNK, body, 0)


def kernel(
    tokens,
    new_rows,
    new_query,
    gain,
    key_weight,
    value_weight,
    input_weight,
    forget_weight,
    bias,
    offsets,
    out_keys,
    out_values,
    out_weights,
    out_read,
    T,
    X,
    N,
    W,
    OK,
    OV,
    G,
    GW,
    NN,
    IG,
    PRE,
    LF,
    S,
    R,
    L,
    LW,
    PEAK,
    Q8,
    NUM,
    DEN,
    KVN,
    GN,
    FS,
    FR,
    A0,
    A1,
    p1s,
    p1r,
    xl,
    xr,
    xf,
    dr,
    xs,
    lws,
    lwr,
    wc,
    wh,
    w2,
    wy,
    ws1,
    ws2,
    fs,
    fr,
    loc,
):
    s = lax.axis_index("sp")
    t = lax.axis_index("tp")
    z, y = s // 4, s % 4
    x, c = t // 2, t % 2
    k_me = s // 8
    n_me = s // 8
    right = ((x + 1) % 4) * 2 + c
    left = ((x + 3) % 4) * 2 + c
    across = ((x + 2) % 4) * 2 + c
    mate = t + 1 - 2 * c

    barrier = pltpu.get_barrier_semaphore()

    def greet(o, carry):
        pl.semaphore_signal(barrier, inc=1, device_id={"sp": (s + o) % 32}, device_id_type=MESH)
        return carry

    lax.fori_loop(1, 32, greet, 0)
    for who in (right, left, mate):
        pl.semaphore_signal(barrier, inc=1, device_id={"tp": who}, device_id_type=MESH)

    own_k = pltpu.make_async_copy(key_weight, W.at[z, y, :, 0:128], loc.at[4])
    own_v = pltpu.make_async_copy(value_weight, W.at[z, y, :, 128:384], loc.at[5])
    own_k.start()
    own_v.start()
    loads = [
        pltpu.make_async_copy(tokens.at[n * GROUP : (n + 1) * GROUP], X.at[n * GROUP : (n + 1) * GROUP], loc.at[n])
        for n in range(4)
    ]
    for load in loads:
        load.start()

    GW[0:16, :] = input_weight[...]
    GW[16:32, :] = forget_weight[...]

    for n in range(4):
        loads[n].wait()

        def gates(n=n):
            norm_group(X, n * GROUP, N, gain)
            G[n] = lax.dot_general(GW[...], N[...], NT, preferred_element_type=F32)

        gates()

    gate_row = iota((32, GROUP), 0)
    for n in range(4):
        for h in range(2):
            at = slice(2 * n + h, 2 * n + h + 1)
            mine = jnp.where(gate_row == 2 * t + h, G[n], 0.0)
            IG[at, :] = jnp.sum(mine, axis=0, keepdims=True) + offsets[n, 0, h : h + 1, :]
            mine = jnp.where(gate_row == 16 + 2 * t + h, G[n], 0.0)
            PRE[at, :] = jnp.sum(mine, axis=0, keepdims=True) + bias[h]
            LF[at, :] = offsets[n, 1, h : h + 1, :]

    lane = iota((8, GROUP), 1)
    pre = PRE[...]
    soft = jnp.minimum(pre, 0.0) - jnp.log1p(jnp.exp(-jnp.abs(pre)))
    log_forget = soft + LF[...]
    suffix = log_forget
    step = 1
    while step < GROUP:
        suffix = suffix + jnp.where(lane < GROUP - step, pltpu.roll(suffix, GROUP - step, 1), 0.0)
        step *= 2
    exclusive = jnp.where(lane < GROUP - 1, pltpu.roll(suffix, GROUP - 1, 1), 0.0)
    local = IG[...] + exclusive
    total = jnp.broadcast_to(suffix[:, 0:1], (8, 128))
    most = jnp.broadcast_to(jnp.max(local, axis=1, keepdims=True), (8, 128))
    lane = iota((8, 128), 1)
    tail_part = jnp.where(
        lane < 80,
        total,
        jnp.where(lane < 96, pltpu.roll(total, 7, 0), jnp.where(lane < 112, most, pltpu.roll(most, 7, 0))),
    )
    for half in range(2):
        part = local[:, half * 128 : (half + 1) * 128]
        for k in range(4):
            first = pltpu.roll(part, (128 - 32 * k) % 128, 1) if k else part
            second = pltpu.roll(pltpu.roll(part, 7, 0), (160 - 32 * k) % 128, 1) if k != 1 else pltpu.roll(part, 7, 0)
            row = jnp.where(lane < 32, first, jnp.where(lane < 64, second, tail_part))
            for n in range(4):
                S[n * 8 + half * 4 + k] = row[2 * n : 2 * n + 1, :]
    R[pl.ds(s, 1)] = S[pl.ds(s, 1)]

    own_k.wait()
    own_v.wait()
    pl.semaphore_wait(barrier, 34)

    half_z = (z // 4) * 4
    other_z = 4 - half_z
    far_z = (z + 4) % 8

    def shard_to(row, to_z, recv):
        pltpu.make_async_remote_copy(
            src_ref=W.at[row, y],
            dst_ref=W.at[row, y],
            send_sem=ws1,
            recv_sem=recv,
            device_id={"sp": to_z * 4 + y},
            device_id_type=MESH,
        ).start()

    shard_to(z, far_z, wc)
    for o in range(1, 4):
        shard_to(z, half_z + (z + o) % 4, wh)

    def send_rows(o, carry):
        peer = (s + o) % 32
        pltpu.make_async_remote_copy(
            src_ref=S.at[peer],
            dst_ref=R.at[s],
            send_sem=lws,
            recv_sem=lwr,
            device_id={"sp": peer},
            device_id_type=MESH,
        ).start()
        return carry

    lax.fori_loop(1, 32, send_rows, 0)

    def slot(i):
        return xor2(k_me, (2 * i + 1) % 5)

    def first_leg(i):
        dest = (t - s + 32) % 8 + 8 * slot(i)
        src = tokens.at[pl.ds(pl.multiple_of(dest * BLOCK, BLOCK), BLOCK)]
        dst = T.at[pl.ds(pl.multiple_of(s * BLOCK, BLOCK), BLOCK)]
        remote = pltpu.make_async_remote_copy(
            src_ref=src,
            dst_ref=dst,
            send_sem=p1s.at[i],
            recv_sem=p1r.at[i],
            device_id={"sp": dest},
            device_id_type=MESH,
        )
        return dest, src, dst, remote

    def start_leg(i, carry):
        dest, src, dst, remote = first_leg(i)

        @pl.when(dest != s)
        def _():
            remote.start()

        @pl.when(dest == s)
        def _():
            pltpu.make_async_copy(src, dst, p1r.at[i]).start()

        return carry

    lax.fori_loop(0, 4, start_leg, 0)

    def y_send(rows, column, to_y, which):
        pltpu.make_async_remote_copy(
            src_ref=W.at[pl.ds(rows, 4), column],
            dst_ref=W.at[pl.ds(rows, 4), column],
            send_sem=ws2,
            recv_sem=wy.at[which],
            device_id={"sp": z * 4 + to_y},
            device_id_type=MESH,
        ).start()

    def arrived(ref, sem):
        pltpu.make_async_copy(ref, ref, sem).wait()

    up, down = (y + 1) % 4, (y + 3) % 4

    arrived(W.at[0, 0], wc)
    for o in range(1, 4):
        shard_to(far_z, half_z + (z + o) % 4, w2)
    arrived(W.at[0:3, 0], wh)
    y_send(half_z, y, up, 0)
    y_send(half_z, y, down, 1)

    arrived(R.at[0:31], lwr)
    received = R[:, 0, :]
    row = iota((32, 128), 0)
    suffix = received
    step = 1
    while step < 32:
        suffix = suffix + jnp.where(row < 32 - step, pltpu.roll(suffix, 32 - step, 0), 0.0)
        step *= 2
    exclusive = jnp.where(row < 31, pltpu.roll(suffix, 31, 0), 0.0)
    tail0, tail1 = exclusive[:, 64:65], exclusive[:, 80:81]
    lane32 = iota((32, 128), 1)
    peak0 = jnp.max(received[:, 96:97] + tail0, axis=0, keepdims=True)
    peak1 = jnp.max(received[:, 112:113] + tail1, axis=0, keepdims=True)
    L[...] = received + jnp.where(lane32 < 32, tail0, tail1)
    even = iota((8, 128), 0) % 2 == 0
    PEAK[...] = jnp.where(even, jnp.broadcast_to(peak0, (8, 128)), jnp.broadcast_to(peak1, (8, 128)))
    for h in range(2):
        wide = jnp.zeros((8, 128), F32)
        for k in range(4):
            rows = L[pl.ds(k, 8, stride=4), :]
            shift = (32 * k - 32 * h) % 128
            moved = pltpu.roll(rows, shift, 1) if shift else rows
            wide = jnp.where((lane >= 32 * k) & (lane < 32 * k + 32), moved, wide)
        for g in range(8):
            LW[h : h + 1, g * 128 : (g + 1) * 128] = wide[g : g + 1, :]
    out_weights[...] = LW[...]

    query = new_query[...].astype(F32)
    lane1 = iota((1, 128), 1)
    for n in range(4):
        Q8[2 * n : 2 * n + 1, :] = jnp.where(lane1 < 64, query[n : n + 1, :], 0.0)
        Q8[2 * n + 1 : 2 * n + 2, :] = jnp.where(lane1 < 64, 0.0, query[n : n + 1, :])

    NUM[...] = jnp.zeros_like(NUM)
    DEN[...] = jnp.zeros_like(DEN)

    def block_of(owner, i):
        at = ((owner - s + 32) % 8 + 8 * slot(i)) * BLOCK
        return T.at[pl.ds(pl.multiple_of(at, BLOCK), BLOCK)]

    def pass_on(owner, i, to, recv):
        block = block_of(owner, i)
        pltpu.make_async_remote_copy(
            src_ref=block,
            dst_ref=block,
            send_sem=xs,
            recv_sem=recv,
            device_id={"tp": to},
            device_id_type=MESH,
        ).start()

    one_block = T.at[0:BLOCK]

    def stage_a(i):
        arrived(one_block, p1r.at[i])
        pass_on(t, i, right, xl.at[i])
        pass_on(t, i, left, xr.at[i])
        pass_on(t, i, mate, dr.at[i])

    def stage_b(i):
        arrived(one_block, xl.at[i])

        @pl.when(i % 2 == 0)
        def _():
            pass_on(left, i, right, xf.at[i])

        pass_on(left, i, mate, dr.at[i])
        arrived(one_block, xr.at[i])

        @pl.when(i % 2 == 1)
        def _():
            pass_on(right, i, left, xf.at[i])

        pass_on(right, i, mate, dr.at[i])

    def stage_c(i):
        arrived(one_block, xf.at[i])
        pass_on(across, i, mate, dr.at[i])

    def write_out(i):
        at = pl.ds(pl.multiple_of(slot(i) * GROUP, GROUP), GROUP)
        return (
            pltpu.make_async_copy(OK.at[at], out_keys.at[at], loc.at[6]),
            pltpu.make_async_copy(OV.at[at], out_values.at[at], loc.at[7]),
        )

    def stage_d(i):
        arrived(T.at[0 : 4 * BLOCK], dr.at[i])
        start = pl.multiple_of(slot(i) * GROUP, GROUP)
        norm_group(T, start, N, gain)
        both = jnp.dot(N[...], W[...].reshape(D, 384), preferred_element_type=F32)
        keys = (both[:, 0:128] * 0.125).astype(BF16)
        values = both[:, 128:384].astype(BF16)
        OK[pl.ds(start, GROUP), :] = keys
        OV[pl.ds(start, GROUP), :] = values
        scores = lax.dot_general(Q8[...].astype(BF16), keys, NT, preferred_element_type=F32)
        weights = LW[:, pl.ds(start, GROUP)]
        rows = iota((8, GROUP), 0)
        weights = jnp.where(rows % 2 == 0, weights[0:1, :], weights[1:2, :])
        terms = jnp.exp(weights - PEAK[:, 0:1]) * scores
        terms = jnp.where(rows // 2 == n_me, terms, 0.0)
        DEN[...] += jnp.broadcast_to(jnp.sum(terms, axis=1, keepdims=True), (8, 128))
        NUM[...] += jnp.dot(terms.astype(BF16), values, preferred_element_type=F32)
        for copy in write_out(i):
            copy.start()

    def along(j, carry):
        @pl.when(j < 4)
        def _():
            stage_a(j)
            stage_b(j)

        @pl.when(j == 0)
        def _():
            arrived(W.at[0:4, 0], wy.at[0])
            y_send(half_z, down, up, 2)
            arrived(W.at[0:3, 0], w2)
            y_send(other_z, y, up, 3)
            y_send(other_z, y, down, 4)

        @pl.when(j == 1)
        def _():
            arrived(W.at[0:4, 0], wy.at[4])
            y_send(other_z, up, down, 5)

        @pl.when((j >= 1) & (j < 5))
        def _():
            stage_c(j - 1)

        @pl.when(j == 2)
        def _():
            for which in (1, 2, 3, 5):
                arrived(W.at[0:4, 0], wy.at[which])
            wide = new_rows[...].astype(F32)
            inverse = lax.rsqrt(jnp.mean(wide * wide, axis=-1, keepdims=True) + EPSILON)
            NN[0:4, :] = wide * inverse * gain[...].astype(F32)
            NN[4:8, :] = jnp.zeros((4, D), F32)
            fresh = NN[...].astype(BF16)
            KVN[...] = jnp.dot(fresh, W[...].reshape(D, 384), preferred_element_type=F32)
            GN[...] = lax.dot_general(fresh, GW[...], NT, preferred_element_type=F32)

        @pl.when(j >= 2)
        def _():
            stage_d(j - 2)

        return carry

    lax.fori_loop(0, 6, along, 0)

    evens = (iota((8, 128), 0) % 2 == 0).astype(F32)
    odds = 1.0 - evens
    FS[0:1, :] = jnp.sum(NUM[:, 0:128] * evens, axis=0, keepdims=True)
    FS[1:2, :] = jnp.sum(NUM[:, 128:256] * odds, axis=0, keepdims=True)
    den0 = jnp.sum(DEN[...] * evens, axis=0, keepdims=True)
    den1 = jnp.sum(DEN[...] * odds, axis=0, keepdims=True)
    FS[2:3, :] = jnp.where(lane1 < 64, den0, den1)
    FS[3:4, :] = jnp.where(lane1 < 64, PEAK[0:1, :], PEAK[1:2, :])
    FR[pl.ds(s, 1)] = FS[...].reshape(1, 4, 128)

    def send_read(o, carry):
        pltpu.make_async_remote_copy(
            src_ref=FS,
            dst_ref=FR.at[s],
            send_sem=fs,
            recv_sem=fr,
            device_id={"sp": (s + o) % 32},
            device_id_type=MESH,
        ).start()
        return carry

    lax.fori_loop(1, 32, send_read, 0)

    own_head = iota((8, 32), 1)
    gate0 = jnp.sum(jnp.where(own_head == 2 * t, GN[...], 0.0), axis=1, keepdims=True)[0:4]
    gate1 = jnp.sum(jnp.where(own_head == 2 * t + 1, GN[...], 0.0), axis=1, keepdims=True)[0:4]
    key_new = (KVN[0:4, 0:128] * 0.125).astype(BF16).astype(F32)
    value_new = KVN[0:4, 128:384].astype(BF16).astype(F32)
    product = query * key_new
    lane4 = iota((4, 128), 1)
    own0 = jnp.sum(jnp.where(lane4 < 64, product, 0.0), axis=1, keepdims=True)
    own1 = jnp.sum(jnp.where(lane4 < 64, 0.0, product), axis=1, keepdims=True)

    arrived(OK, loc.at[6])
    arrived(OV, loc.at[7])

    arrived(FR.at[0:31], fr)
    for n in range(4):
        group = FR[n * 8 : n * 8 + 8]
        added = jnp.sum(group, axis=0)
        A0[n : n + 1, :] = added[0:1, :]
        A0[4 + n : 5 + n, :] = added[1:2, :]
        A1[n : n + 1, :] = added[2:3, :]
        A1[4 + n : 5 + n, :] = group[0, 3:4, :]

    for h, (gate, own) in enumerate(((gate0, own0), (gate1, own1))):
        numerator = A0[4 * h : 4 * h + 4, :]
        denominator = A1[0:4, 64 * h : 64 * h + 1]
        peak = A1[4:8, 64 * h : 64 * h + 1]
        top = jnp.maximum(peak, gate)
        old_part = jnp.exp(peak - top)
        new_part = jnp.exp(gate - top) * own
        value = old_part * numerator + new_part * value_new[:, h * 128 : (h + 1) * 128]
        weight = old_part * denominator + new_part
        out_read[:, h * 128 : (h + 1) * 128] = (value / jnp.maximum(jnp.abs(weight), 1.0)).astype(BF16)

    arrived(R.at[0:31], lws)
    arrived(FR.at[0:31], fs)
    arrived(W.at[0:7, 0], ws1)
    arrived(W.at[0:6], ws2)
    arrived(T.at[0 : 28 * BLOCK], xs)

    def leg_done(i, carry):
        dest, _, _, remote = first_leg(i)

        @pl.when(dest != s)
        def _():
            remote.wait_send()

        return carry

    lax.fori_loop(0, 4, leg_done, 0)


def per_device(
    tokens,
    new_rows,
    new_query,
    norm_gain,
    key_weight,
    value_weight,
    input_weight,
    forget_weight,
    forget_bias,
    gate_offsets,
):
    any_space = pl.BlockSpec(memory_space=pl.ANY)
    vmem = pl.BlockSpec(memory_space=pltpu.VMEM)
    smem = pl.BlockSpec(memory_space=pltpu.SMEM)
    dma = pltpu.SemaphoreType.DMA
    keys, values, weights, read = pl.pallas_call(
        kernel,
        out_shape=(
            jax.ShapeDtypeStruct((ROWS, 128), BF16),
            jax.ShapeDtypeStruct((ROWS, 256), BF16),
            jax.ShapeDtypeStruct((2, ROWS), F32),
            jax.ShapeDtypeStruct((4, 256), BF16),
        ),
        in_specs=[any_space, vmem, vmem, vmem, any_space, any_space, vmem, vmem, smem, vmem],
        out_specs=(any_space, any_space, vmem, vmem),
        scratch_shapes=[
            pltpu.VMEM((ROWS, D), BF16),
            pltpu.VMEM((ROWS, D), BF16),
            pltpu.VMEM((GROUP, D), BF16),
            pltpu.VMEM((8, 4, 64, 384), BF16),
            pltpu.VMEM((ROWS, 128), BF16),
            pltpu.VMEM((ROWS, 256), BF16),
            pltpu.VMEM((4, 32, GROUP), F32),
            pltpu.VMEM((32, D), BF16),
            pltpu.VMEM((8, D), F32),
            pltpu.VMEM((8, GROUP), F32),
            pltpu.VMEM((8, GROUP), F32),
            pltpu.VMEM((8, GROUP), F32),
            pltpu.VMEM((32, 1, 128), F32),
            pltpu.VMEM((32, 1, 128), F32),
            pltpu.VMEM((32, 128), F32),
            pltpu.VMEM((2, ROWS), F32),
            pltpu.VMEM((8, 128), F32),
            pltpu.VMEM((8, 128), F32),
            pltpu.VMEM((8, 256), F32),
            pltpu.VMEM((8, 128), F32),
            pltpu.VMEM((8, 384), F32),
            pltpu.VMEM((8, 32), F32),
            pltpu.VMEM((4, 128), F32),
            pltpu.VMEM((32, 4, 128), F32),
            pltpu.VMEM((8, 128), F32),
            pltpu.VMEM((8, 128), F32),
            dma((4,)),
            dma((4,)),
            dma((4,)),
            dma((4,)),
            dma((4,)),
            dma((4,)),
            dma,
            dma,
            dma,
            dma,
            dma,
            dma,
            dma((6,)),
            dma,
            dma,
            dma,
            dma,
            dma((8,)),
        ],
        compiler_params=pltpu.CompilerParams(collective_id=0, has_side_effects=True),
    )(
        tokens.reshape(ROWS, D),
        new_rows,
        new_query,
        norm_gain.reshape(1, D),
        key_weight,
        value_weight,
        input_weight.T,
        forget_weight.T,
        forget_bias,
        jnp.transpose(gate_offsets, (0, 2, 3, 1)),
    )
    return keys[None], values[None], weights[None], read


def solution(mesh):
    return jax.shard_map(
        per_device,
        mesh=mesh,
        in_specs=(
            P("gr", "sp", None),
            P("gr", None),
            P("gr", "tp"),
            P(),
            P("sp", "tp"),
            P("sp", "tp"),
            P(),
            P(),
            P("tp"),
            P("gr", "sp", None, "tp"),
        ),
        out_specs=(
            P(("gr", "sp"), None, "tp"),
            P(("gr", "sp"), None, "tp"),
            P(("gr", "sp"), "tp", None),
            P("gr", "tp"),
        ),
        check_vma=False,
    )
```

time: 314 us -> 93 us (0.30)
  the two profiles are of different devices: /device:TPU:2 before, /device:TPU:1 now
where the time goes in v1:
time: 93 us; the launch traced here: 91.3 us
  Pallas kernels  83.3 us (90%)
  local copies, waits for them, and re-layouts  7.36 us (8%)
    pallas_call x1, Pallas kernels, per_device(): pl.pallas_call(kernel, out_shape=(jax.ShapeDtypeStruct((ROWS, 128), BF16)...  83.3 us
    unnamed x4, local copies, waits for them, and re-layouts  6.07 us

profile of v1, /device:TPU:1, one launch (start us, length us, event | category | flops | bytes accessed | tf_op | source)
XLA Modules:
  0.0 91.3 jit_solution(889773116533759478)
XLA Ops:
  0.6 1.3 %reshape.15.gain = bf16[1,2048]{1,0:T(2,128)(2,1)} reshape(bf16[2048]{0:T(1024)(128)(2,1)} %param.13) | data formatting | bytes 8192 | tf_op jit(solution)/shard_map/reshape | solution.py:590
  1.9 83.3 %shard_map.129 = (bf16[1024,128]{1,0:T(8,128)(2,1)}, bf16[1024,256]{1,0:T(8,128)(2,1)}, f32[2,1024]{1,0:T(2,128)}, bf16[4,256]{1,0:T(4,128)(2,1)}) custom-call(bf16[1024,2048]{1,0:T(8,128)(2,1)} %bitcast.7, bf16[4,2048]{1,0:T(4,128)(2,1)} %new_rows.1, bf16[4,128]{1,0:T(4,128)(2,1)} %new_query.1, bf16[1,2048]{1,0:T(2,128)(2,1)} %reshape.15.gain, ...), custom_call_target="tpu_custom_call" | custom-call | tf_op jit(solution)/shard_map/pallas_call | solution.py:529
  85.3 1.7 %copy.18 = bf16[1,1024,128]{2,1,0:T(8,128)(2,1)} copy(bf16[1,1024,128]{2,1,0:T(8,128)(2,1)} %bitcast.9) | data formatting | bytes 524288
  86.9 1.9 %copy.19 = bf16[1,1024,256]{2,1,0:T(8,128)(2,1)} copy(bf16[1,1024,256]{2,1,0:T(8,128)(2,1)} %bitcast.8) | data formatting | bytes 1048576
  88.8 1.3 %copy.20 = f32[1,2,1024]{2,1,0:T(2,128)} copy(f32[1,2,1024]{2,1,0:T(2,128)} %bitcast.13) | data formatting | bytes 16384
  90.1 1.2 %copy.21 = bf16[4,256]{1,0:T(4,128)(2,1)} copy(bf16[4,256]{1,0:T(4,128)(2,1)} %get-tuple-element.19) | data formatting | bytes 4096

commit v2 on v1

--- a/solution.py
+++ b/solution.py
@@ -34,7 +34,7 @@
     inverse = lax.rsqrt(jnp.sum(total, axis=-1, keepdims=True) * (1.0 / D) + EPSILON)
     for c in range(D // 128):
         v = read(c).astype(F32)
-        write(c, (v * inverse * gain_ref[:, c * 128 : (c + 1) * 128].astype(F32)).astype(BF16))
+        write(c, (v * inverse * gain_ref[c : c + 1, :].astype(F32)).astype(BF16))
 
 
 def norm_group(src, start, dst, gain_ref):
@@ -56,19 +56,23 @@
 
 def kernel(
     tokens,
-    new_rows,
-    new_query,
-    gain,
+    new_rows_in,
+    new_query_in,
+    gain_in,
     key_weight,
     value_weight,
     input_weight,
     forget_weight,
     bias,
-    offsets,
+    offsets_in,
     out_keys,
     out_values,
     out_weights,
     out_read,
+    new_rows,
+    new_query,
+    gain,
+    offsets,
     T,
     X,
     N,
@@ -143,12 +147,79 @@
         pltpu.make_async_copy(tokens.at[n * GROUP : (n + 1) * GROUP], X.at[n * GROUP : (n + 1) * GROUP], loc.at[n])
         for n in range(4)
     ]
-    for load in loads:
+    loads[0].start()
+    small = [
+        pltpu.make_async_copy(src, dst, loc.at[8 + at])
+        for at, (src, dst) in enumerate(
+            (
+                (gain_in, gain),
+                (input_weight, GW.at[0:16]),
+                (forget_weight, GW.at[16:32]),
+                (offsets_in, offsets),
+                (new_rows_in, new_rows),
+                (new_query_in, new_query),
+            )
+        )
+    ]
+    for copy in small:
+        copy.start()
+    for load in loads[1:]:
         load.start()
-
-    GW[0:16, :] = input_weight[...]
-    GW[16:32, :] = forget_weight[...]
-
+    own_k.wait()
+    own_v.wait()
+    pl.semaphore_wait(barrier, 34)
+
+    half_z = (z // 4) * 4
+    other_z = 4 - half_z
+    far_z = (z + 4) % 8
+
+    def shard_to(row, to_z, recv):
+        pltpu.make_async_remote_copy(
+            src_ref=W.at[row, y],
+            dst_ref=W.at[row, y],
+            send_sem=ws1,
+            recv_sem=recv,
+            device_id={"sp": to_z * 4 + y},
+            device_id_type=MESH,
+        ).start()
+
+    shard_to(z, far_z, wc)
+    for o in range(1, 4):
+        shard_to(z, half_z + (z + o) % 4, wh)
+
+    def slot(i):
+        return xor2(k_me, (2 * i + 1) % 5)
+
+    def first_leg(i):
+        dest = (t - s + 32) % 8 + 8 * slot(i)
+        src = tokens.at[pl.ds(pl.multiple_of(dest * BLOCK, BLOCK), BLOCK)]
+        dst = T.at[pl.ds(pl.multiple_of(s * BLOCK, BLOCK), BLOCK)]
+        remote = pltpu.make_async_remote_copy(
+            src_ref=src,
+            dst_ref=dst,
+            send_sem=p1s.at[i],
+            recv_sem=p1r.at[i],
+            device_id={"sp": dest},
+            device_id_type=MESH,
+        )
+        return dest, src, dst, remote
+
+    def start_leg(i):
+        dest, src, dst, remote = first_leg(i)
+
+        @pl.when(dest != s)
+        def _():
+            remote.start()
+
+        @pl.when(dest == s)
+        def _():
+            pltpu.make_async_copy(src, dst, p1r.at[i]).start()
+
+    start_leg(0)
+    start_leg(1)
+
+    for copy in small:
+        copy.wait()
     for n in range(4):
         loads[n].wait()
 
@@ -197,28 +268,6 @@
                 S[n * 8 + half * 4 + k] = row[2 * n : 2 * n + 1, :]
     R[pl.ds(s, 1)] = S[pl.ds(s, 1)]
 
-    own_k.wait()
-    own_v.wait()
-    pl.semaphore_wait(barrier, 34)
-
-    half_z = (z // 4) * 4
-    other_z = 4 - half_z
-    far_z = (z + 4) % 8
-
-    def shard_to(row, to_z, recv):
-        pltpu.make_async_remote_copy(
-            src_ref=W.at[row, y],
-            dst_ref=W.at[row, y],
-            send_sem=ws1,
-            recv_sem=recv,
-            device_id={"sp": to_z * 4 + y},
-            device_id_type=MESH,
-        ).start()
-
-    shard_to(z, far_z, wc)
-    for o in range(1, 4):
-        shard_to(z, half_z + (z + o) % 4, wh)
-
     def send_rows(o, carry):
         peer = (s + o) % 32
         pltpu.make_async_remote_copy(
@@ -233,38 +282,6 @@
 
     lax.fori_loop(1, 32, send_rows, 0)
 
-    def slot(i):
-        return xor2(k_me, (2 * i + 1) % 5)
-
-    def first_leg(i):
-        dest = (t - s + 32) % 8 + 8 * slot(i)
-        src = tokens.at[pl.ds(pl.multiple_of(dest * BLOCK, BLOCK), BLOCK)]
-        dst = T.at[pl.ds(pl.multiple_of(s * BLOCK, BLOCK), BLOCK)]
-        remote = pltpu.make_async_remote_copy(
-            src_ref=src,
-            dst_ref=dst,
-            send_sem=p1s.at[i],
-            recv_sem=p1r.at[i],
-            device_id={"sp": dest},
-            device_id_type=MESH,
-        )
-        return dest, src, dst, remote
-
-    def start_leg(i, carry):
-        dest, src, dst, remote = first_leg(i)
-
-        @pl.when(dest != s)
-        def _():
-            remote.start()
-
-        @pl.when(dest == s)
-        def _():
-            pltpu.make_async_copy(src, dst, p1r.at[i]).start()
-
-        return carry
-
-    lax.fori_loop(0, 4, start_leg, 0)
-
     def y_send(rows, column, to_y, which):
         pltpu.make_async_remote_copy(
             src_ref=W.at[pl.ds(rows, 4), column],
@@ -286,42 +303,6 @@
     arrived(W.at[0:3, 0], wh)
     y_send(half_z, y, up, 0)
     y_send(half_z, y, down, 1)
-
-    arrived(R.at[0:31], lwr)
-    received = R[:, 0, :]
-    row = iota((32, 128), 0)
-    suffix = received
-    step = 1
-    while step < 32:
-        suffix = suffix + jnp.where(row < 32 - step, pltpu.roll(suffix, 32 - step, 0), 0.0)
-        step *= 2
-    exclusive = jnp.where(row < 31, pltpu.roll(suffix, 31, 0), 0.0)
-    tail0, tail1 = exclusive[:, 64:65], exclusive[:, 80:81]
-    lane32 = iota((32, 128), 1)
-    peak0 = jnp.max(received[:, 96:97] + tail0, axis=0, keepdims=True)
-    peak1 = jnp.max(received[:, 112:113] + tail1, axis=0, keepdims=True)
-    L[...] = received + jnp.where(lane32 < 32, tail0, tail1)
-    even = iota((8, 128), 0) % 2 == 0
-    PEAK[...] = jnp.where(even, jnp.broadcast_to(peak0, (8, 128)), jnp.broadcast_to(peak1, (8, 128)))
-    for h in range(2):
-        wide = jnp.zeros((8, 128), F32)
-        for k in range(4):
-            rows = L[pl.ds(k, 8, stride=4), :]
-            shift = (32 * k - 32 * h) % 128
-            moved = pltpu.roll(rows, shift, 1) if shift else rows
-            wide = jnp.where((lane >= 32 * k) & (lane < 32 * k + 32), moved, wide)
-        for g in range(8):
-            LW[h : h + 1, g * 128 : (g + 1) * 128] = wide[g : g + 1, :]
-    out_weights[...] = LW[...]
-
-    query = new_query[...].astype(F32)
-    lane1 = iota((1, 128), 1)
-    for n in range(4):
-        Q8[2 * n : 2 * n + 1, :] = jnp.where(lane1 < 64, query[n : n + 1, :], 0.0)
-        Q8[2 * n + 1 : 2 * n + 2, :] = jnp.where(lane1 < 64, 0.0, query[n : n + 1, :])
-
-    NUM[...] = jnp.zeros_like(NUM)
-    DEN[...] = jnp.zeros_like(DEN)
 
     def block_of(owner, i):
         at = ((owner - s + 32) % 8 + 8 * slot(i)) * BLOCK
@@ -338,6 +319,20 @@
             device_id_type=MESH,
         ).start()
 
+    half_block = BLOCK // 2
+
+    def pass_half(owner, i, half, to):
+        at = ((owner - s + 32) % 8 + 8 * slot(i)) * BLOCK + half * half_block
+        part = T.at[pl.ds(pl.multiple_of(at, half_block), half_block)]
+        pltpu.make_async_remote_copy(
+            src_ref=part,
+            dst_ref=part,
+            send_sem=xs,
+            recv_sem=xf.at[i, half],
+            device_id={"tp": to},
+            device_id_type=MESH,
+        ).start()
+
     one_block = T.at[0:BLOCK]
 
     def stage_a(i):
@@ -348,22 +343,15 @@
 
     def stage_b(i):
         arrived(one_block, xl.at[i])
-
-        @pl.when(i % 2 == 0)
-        def _():
-            pass_on(left, i, right, xf.at[i])
-
+        pass_half(left, i, 0, right)
         pass_on(left, i, mate, dr.at[i])
         arrived(one_block, xr.at[i])
-
-        @pl.when(i % 2 == 1)
-        def _():
-            pass_on(right, i, left, xf.at[i])
-
+        pass_half(right, i, 1, left)
         pass_on(right, i, mate, dr.at[i])
 
     def stage_c(i):
-        arrived(one_block, xf.at[i])
+        arrived(T.at[0:half_block], xf.at[i, 0])
+        arrived(T.at[0:half_block], xf.at[i, 1])
         pass_on(across, i, mate, dr.at[i])
 
     def write_out(i):
@@ -393,48 +381,89 @@
         for copy in write_out(i):
             copy.start()
 
-    def along(j, carry):
-        @pl.when(j < 4)
-        def _():
-            stage_a(j)
-            stage_b(j)
-
-        @pl.when(j == 0)
-        def _():
-            arrived(W.at[0:4, 0], wy.at[0])
-            y_send(half_z, down, up, 2)
-            arrived(W.at[0:3, 0], w2)
-            y_send(other_z, y, up, 3)
-            y_send(other_z, y, down, 4)
-
-        @pl.when(j == 1)
-        def _():
-            arrived(W.at[0:4, 0], wy.at[4])
-            y_send(other_z, up, down, 5)
-
-        @pl.when((j >= 1) & (j < 5))
-        def _():
-            stage_c(j - 1)
-
-        @pl.when(j == 2)
-        def _():
-            for which in (1, 2, 3, 5):
-                arrived(W.at[0:4, 0], wy.at[which])
-            wide = new_rows[...].astype(F32)
-            inverse = lax.rsqrt(jnp.mean(wide * wide, axis=-1, keepdims=True) + EPSILON)
-            NN[0:4, :] = wide * inverse * gain[...].astype(F32)
-            NN[4:8, :] = jnp.zeros((4, D), F32)
-            fresh = NN[...].astype(BF16)
-            KVN[...] = jnp.dot(fresh, W[...].reshape(D, 384), preferred_element_type=F32)
-            GN[...] = lax.dot_general(fresh, GW[...], NT, preferred_element_type=F32)
-
-        @pl.when(j >= 2)
-        def _():
-            stage_d(j - 2)
-
-        return carry
-
-    lax.fori_loop(0, 6, along, 0)
+    def log_weights():
+        arrived(R.at[0:31], lwr)
+        received = R[:, 0, :]
+        row = iota((32, 128), 0)
+        suffix = received
+        step = 1
+        while step < 32:
+            suffix = suffix + jnp.where(row < 32 - step, pltpu.roll(suffix, 32 - step, 0), 0.0)
+            step *= 2
+        exclusive = jnp.where(row < 31, pltpu.roll(suffix, 31, 0), 0.0)
+        tail0, tail1 = exclusive[:, 64:65], exclusive[:, 80:81]
+        lane32 = iota((32, 128), 1)
+        peak0 = jnp.max(received[:, 96:97] + tail0, axis=0, keepdims=True)
+        peak1 = jnp.max(received[:, 112:113] + tail1, axis=0, keepdims=True)
+        L[...] = received + jnp.where(lane32 < 32, tail0, tail1)
+        even = iota((8, 128), 0) % 2 == 0
+        PEAK[...] = jnp.where(even, jnp.broadcast_to(peak0, (8, 128)), jnp.broadcast_to(peak1, (8, 128)))
+        for h in range(2):
+            wide = jnp.zeros((8, 128), F32)
+            for k in range(4):
+                rows = L[pl.ds(k, 8, stride=4), :]
+                shift = (32 * k - 32 * h) % 128
+                moved = pltpu.roll(rows, shift, 1) if shift else rows
+                wide = jnp.where((lane >= 32 * k) & (lane < 32 * k + 32), moved, wide)
+            for g in range(8):
+                LW[h : h + 1, g * 128 : (g + 1) * 128] = wide[g : g + 1, :]
+        out_weights[...] = LW[...]
+
+        query = new_query[...].astype(F32)
+        for n in range(4):
+            Q8[2 * n : 2 * n + 1, :] = jnp.where(lane1 < 64, query[n : n + 1, :], 0.0)
+            Q8[2 * n + 1 : 2 * n + 2, :] = jnp.where(lane1 < 64, 0.0, query[n : n + 1, :])
+
+        NUM[...] = jnp.zeros_like(NUM)
+        DEN[...] = jnp.zeros_like(DEN)
+
+    query = new_query[...].astype(F32)
+    lane1 = iota((1, 128), 1)
+    lane = iota((8, 128), 1)
+
+    def new_row_parts():
+        total = jnp.zeros((4, 128), F32)
+        for g in range(D // 128):
+            v = new_rows[:, g * 128 : (g + 1) * 128].astype(F32)
+            total = total + v * v
+        inverse = lax.rsqrt(jnp.sum(total, axis=-1, keepdims=True) * (1.0 / D) + EPSILON)
+        NN[...] = jnp.zeros_like(NN)
+        for g in range(D // 128):
+            at = slice(g * 128, (g + 1) * 128)
+            NN[0:4, at] = new_rows[:, at].astype(F32) * inverse * gain[g : g + 1, :].astype(F32)
+        fresh = NN[...].astype(BF16)
+        KVN[...] = jnp.dot(fresh, W[...].reshape(D, 384), preferred_element_type=F32)
+        GN[...] = lax.dot_general(fresh, GW[...], NT, preferred_element_type=F32)
+
+    stage_a(0)
+    start_leg(2)
+    arrived(W.at[0:4, 0], wy.at[0])
+    y_send(half_z, down, up, 2)
+    arrived(W.at[0:3, 0], w2)
+    y_send(other_z, y, up, 3)
+    y_send(other_z, y, down, 4)
+    stage_b(0)
+    log_weights()
+    stage_a(2)
+    stage_a(1)
+    start_leg(3)
+    arrived(W.at[0:4, 0], wy.at[4])
+    y_send(other_z, up, down, 5)
+    stage_c(0)
+    stage_b(2)
+    stage_b(1)
+    stage_c(2)
+    stage_c(1)
+    for which in (1, 2, 3, 5):
+        arrived(W.at[0:4, 0], wy.at[which])
+    new_row_parts()
+    stage_d(0)
+    stage_a(3)
+    stage_d(2)
+    stage_b(3)
+    stage_d(1)
+    stage_c(3)
+    stage_d(3)
 
     evens = (iota((8, 128), 0) % 2 == 0).astype(F32)
     odds = 1.0 - evens
@@ -508,6 +537,19 @@
         return carry
 
     lax.fori_loop(0, 4, leg_done, 0)
+
+
+def place(keys, values, weights, read, out_keys, out_values, out_weights, out_read, sems):
+    copies = [
+        pltpu.make_async_copy(keys, out_keys.at[0], sems.at[0]),
+        pltpu.make_async_copy(values, out_values.at[0], sems.at[1]),
+        pltpu.make_async_copy(weights, out_weights.at[0], sems.at[2]),
+        pltpu.make_async_copy(read, out_read, sems.at[3]),
+    ]
+    for copy in copies:
+        copy.start()
+    for copy in copies:
+        copy.wait()
 
 
 def per_device(
@@ -534,9 +576,13 @@
             jax.ShapeDtypeStruct((2, ROWS), F32),
             jax.ShapeDtypeStruct((4, 256), BF16),
         ),
-        in_specs=[any_space, vmem, vmem, vmem, any_space, any_space, vmem, vmem, smem, vmem],
+        in_specs=[any_space] * 8 + [smem, any_space],
         out_specs=(any_space, any_space, vmem, vmem),
         scratch_shapes=[
+            pltpu.VMEM((4, D), BF16),
+            pltpu.VMEM((4, 128), BF16),
+            pltpu.VMEM((16, 128), BF16),
+            pltpu.VMEM((4, 2, 2, GROUP), F32),
             pltpu.VMEM((ROWS, D), BF16),
             pltpu.VMEM((ROWS, D), BF16),
             pltpu.VMEM((GROUP, D), BF16),
@@ -567,8 +613,8 @@
             dma((4,)),
             dma((4,)),
             dma((4,)),
+            dma((4, 2)),
             dma((4,)),
-            dma((4,)),
             dma,
             dma,
             dma,
@@ -580,14 +626,14 @@
             dma,
             dma,
             dma,
-            dma((8,)),
+            dma((14,)),
         ],
         compiler_params=pltpu.CompilerParams(collective_id=0, has_side_effects=True),
     )(
         tokens.reshape(ROWS, D),
         new_rows,
         new_query,
-        norm_gain.reshape(1, D),
+        norm_gain.reshape(16, 128),
         key_weight,
         value_weight,
         input_weight.T,
@@ -595,7 +641,18 @@
         forget_bias,
         jnp.transpose(gate_offsets, (0, 2, 3, 1)),
     )
-    return keys[None], values[None], weights[None], read
+    return pl.pallas_call(
+        place,
+        out_shape=(
+            jax.ShapeDtypeStruct((1, ROWS, 128), BF16),
+            jax.ShapeDtypeStruct((1, ROWS, 256), BF16),
+            jax.ShapeDtypeStruct((1, 2, ROWS), F32),
+            jax.ShapeDtypeStruct((4, 256), BF16),
+        ),
+        in_specs=[vmem] * 4,
+        out_specs=[any_space] * 4,
+        scratch_shapes=[dma((4,))],
+    )(keys, values, weights, read)
 
 
 def solution(mesh):

time: 93 us -> 79 us (0.85); the launches traced: 91.3 us -> 78.8 us
  local copies, waits for them, and re-layouts: 7.36 us -> 0 us
  Pallas kernels: 83.3 us -> 78.2 us
    pallas_call x1, Pallas kernels: 83.3 us -> 76.1 us  [per_device(): pl.pallas_call(kernel, out_shape=(jax.ShapeDtypeStruct((ROWS, 128), BF16)...]
    unnamed x4 -> x0, local copies, waits for them, and re-layouts: 6.07 us -> none
    pallas_call x0 -> x1, Pallas kernels: none -> 2.03 us  [per_device(): pl.pallas_call(place, out_shape=(jax.ShapeDtypeStruct((1, ROWS, 128), BF1...]
    reshape x1 -> x0, local copies, waits for them, and re-layouts: 1.29 us -> none  [per_device(): norm_gain.reshape(1, D)]
where the time goes in v2:
time: 79 us; the launch traced here: 78.8 us
  Pallas kernels  78.2 us (99%)
    pallas_call x1, Pallas kernels, per_device(): pl.pallas_call(kernel, out_shape=(jax.ShapeDtypeStruct((ROWS, 128), BF16)...  76.1 us
    pallas_call x1, Pallas kernels, per_device(): pl.pallas_call(place, out_shape=(jax.ShapeDtypeStruct((1, ROWS, 128), BF1...  2.03 us

profile of v2, /device:TPU:1, one launch (start us, length us, event | category | flops | bytes accessed | tf_op | source)
XLA Modules:
  0.0 78.8 jit_solution(6172300065885095729)
XLA Ops:
  0.6 76.1 %shard_map.129 = (bf16[1024,128]{1,0:T(8,128)(2,1)}, bf16[1024,256]{1,0:T(8,128)(2,1)}, f32[2,1024]{1,0:T(2,128)}, bf16[4,256]{1,0:T(4,128)(2,1)}) custom-call(bf16[1024,2048]{1,0:T(8,128)(2,1)} %bitcast.5, bf16[4,2048]{1,0:T(4,128)(2,1)} %new_rows_in.1, bf16[4,128]{1,0:T(4,128)(2,1)} %new_query_in.1, bf16[16,128]{1,0:T(8,128)(2,1)} %bitcast.9, ...), custom_call_target="tpu_custom_call" | custom-call | tf_op jit(solution)/shard_map/pallas_call | solution.py:571
  76.8 2.0 %shard_map.130 = (bf16[1,1024,128]{2,1,0:T(8,128)(2,1)}, bf16[1,1024,256]{2,1,0:T(8,128)(2,1)}, f32[1,2,1024]{2,1,0:T(2,128)}, bf16[4,256]{1,0:T(4,128)(2,1)}) custom-call(bf16[1024,128]{1,0:T(8,128)(2,1)} %get-tuple-element.8.keys, bf16[1024,256]{1,0:T(8,128)(2,1)} %get-tuple-element.9.values, f32[2,1024]{1,0:T(2,128)} %get-tuple-element.10.weights, ...), custom_call_target="tpu_custom_call" | custom-call | tf_op jit(solution)/shard_map/pallas_call | solution.py:644

commit v3 on v2

v3 whole, which is shorter than its diff:
```python
import jax
import jax.numpy as jnp
from jax import lax
from jax.experimental import pallas as pl
from jax.experimental.pallas import tpu as pltpu
from jax.sharding import PartitionSpec as P

EPSILON = 1e-06
MESH = pl.DeviceIdType.MESH
F32 = jnp.float32
BF16 = jnp.bfloat16
NT = (((1,), (1,)), ((), ()))

D = 2048
ROWS = 1024
GROUP = 256
BLOCK = 32
CHUNK = 64


def iota(shape, dim):
    return lax.broadcasted_iota(jnp.int32, shape, dim)


def xor2(a, b):
    return 2 * ((a // 2 + b // 2) % 2) + (a % 2 + b % 2) % 2


def norm_chunk(read, write, gain_ref, rows):
    total = jnp.zeros((rows, 128), F32)
    for c in range(D // 128):
        v = read(c).astype(F32)
        total = total + v * v
    inverse = lax.rsqrt(jnp.sum(total, axis=-1, keepdims=True) * (1.0 / D) + EPSILON)
    for c in range(D // 128):
        v = read(c).astype(F32)
        write(c, (v * inverse * gain_ref[c : c + 1, :].astype(F32)).astype(BF16))


def norm_group(src, start, dst, first, gain_ref):
    def body(u, carry):
        at = pl.multiple_of(start + u * CHUNK, CHUNK)
        to = pl.multiple_of(first + u * CHUNK, CHUNK)

        def read(c):
            return src[pl.ds(at, CHUNK), c * 128 : (c + 1) * 128]

        def write(c, v):
            dst[pl.ds(to, CHUNK), c * 128 : (c + 1) * 128] = v

        norm_chunk(read, write, gain_ref, CHUNK)
        return carry

    lax.fori_loop(0, GROUP // CHUNK, body, 0)


def kernel(
    tokens,
    new_rows_in,
    new_query_in,
    gain_in,
    key_weight,
    value_weight,
    input_weight,
    forget_weight,
    bias,
    offsets_in,
    out_keys,
    out_values,
    out_weights,
    out_read,
    new_rows,
    new_query,
    gain,
    offsets,
    T,
    X,
    N,
    W,
    OK,
    OV,
    G,
    GW,
    NN,
    IG,
    PRE,
    LF,
    LOC,
    S,
    R,
    L,
    LW,
    PEAK,
    Q8,
    NUM,
    DEN,
    KN8,
    VN8,
    GN8,
    E1,
    E2,
    A0,
    p1s,
    p1r,
    xl,
    xr,
    xf,
    dr,
    xs,
    lws,
    lwr,
    wc,
    wh,
    w2,
    wy,
    ws1,
    ws2,
    es,
    er,
    loc,
):
    s = lax.axis_index("sp")
    t = lax.axis_index("tp")
    z, y = s // 4, s % 4
    x, c = t // 2, t % 2
    k_me = s // 8
    n_me = s // 8
    right = ((x + 1) % 4) * 2 + c
    left = ((x + 3) % 4) * 2 + c
    across = ((x + 2) % 4) * 2 + c
    mate = t + 1 - 2 * c

    barrier = pltpu.get_barrier_semaphore()

    def greet(o, carry):
        pl.semaphore_signal(barrier, inc=1, device_id={"sp": (s + o) % 32}, device_id_type=MESH)
        return carry

    lax.fori_loop(1, 32, greet, 0)
    for who in (right, left, mate):
        pl.semaphore_signal(barrier, inc=1, device_id={"tp": who}, device_id_type=MESH)

    own_k = pltpu.make_async_copy(key_weight, W.at[z, y, :, 0:128], loc.at[4])
    own_v = pltpu.make_async_copy(value_weight, W.at[z, y, :, 128:384], loc.at[5])
    own_k.start()
    own_v.start()
    loads = [
        pltpu.make_async_copy(tokens.at[n * GROUP : (n + 1) * GROUP], X.at[n * GROUP : (n + 1) * GROUP], loc.at[n])
        for n in range(4)
    ]
    loads[0].start()
    small = [
        pltpu.make_async_copy(src, dst, loc.at[8 + at])
        for at, (src, dst) in enumerate(
            (
                (gain_in, gain),
                (input_weight, GW.at[0:16]),
                (forget_weight, GW.at[16:32]),
                (offsets_in, offsets),
                (new_rows_in, new_rows),
                (new_query_in, new_query),
            )
        )
    ]
    for copy in small:
        copy.start()
    for load in loads[1:]:
        load.start()
    own_k.wait()
    own_v.wait()
    pl.semaphore_wait(barrier, 34)

    half_z = (z // 4) * 4
    other_z = 4 - half_z
    far_z = (z + 4) % 8

    def shard_to(row, to_z, recv):
        pltpu.make_async_remote_copy(
            src_ref=W.at[row, y],
            dst_ref=W.at[row, y],
            send_sem=ws1,
            recv_sem=recv,
            device_id={"sp": to_z * 4 + y},
            device_id_type=MESH,
        ).start()

    inner = (k_me // 2 + k_me % 2) % 2

    def sent_at(j):
        return inner * (0, 1, 2, 3)[j] + (1 - inner) * (0, 3, 2, 1)[j]

    def due_at(j):
        return inner * (0, 2, 1, 3)[j] + (1 - inner) * (0, 1, 3, 2)[j]

    def slot(i):
        return xor2(k_me, i)

    def first_leg(i):
        dest = (t - s + i + 32) % 8 + 8 * slot(i)
        src = tokens.at[pl.ds(pl.multiple_of(dest * BLOCK, BLOCK), BLOCK)]
        dst = T.at[pl.ds(pl.multiple_of(s * BLOCK, BLOCK), BLOCK)]
        remote = pltpu.make_async_remote_copy(
            src_ref=src,
            dst_ref=dst,
            send_sem=p1s.at[i],
            recv_sem=p1r.at[i],
            device_id={"sp": dest},
            device_id_type=MESH,
        )
        return dest, src, dst, remote

    def start_leg(j):
        i = sent_at(j)
        dest, src, dst, remote = first_leg(i)

        @pl.when(dest != s)
        def _():
            remote.start()

        @pl.when(dest == s)
        def _():
            pltpu.make_async_copy(src, dst, p1r.at[i]).start()

    shard_to(z, far_z, wc)
    for o in range(1, 4):
        shard_to(z, half_z + (z + o) % 4, wh)

    start_leg(0)

    def y_send(rows, column, to_y, which):
        pltpu.make_async_remote_copy(
            src_ref=W.at[pl.ds(rows, 4), column],
            dst_ref=W.at[pl.ds(rows, 4), column],
            send_sem=ws2,
            recv_sem=wy.at[which],
            device_id={"sp": z * 4 + to_y},
            device_id_type=MESH,
        ).start()

    def arrived(ref, sem):
        pltpu.make_async_copy(ref, ref, sem).wait()

    up, down = (y + 1) % 4, (y + 3) % 4

    def gates(n):
        loads[n].wait()
        norm_group(X, n * GROUP, X, n * GROUP, gain)
        own = X[n * GROUP : (n + 1) * GROUP, :]
        G[n] = lax.dot_general(GW[...], own, NT, preferred_element_type=F32)

    lane = iota((8, 128), 1)
    head_row = iota((8, 128), 0)

    def local_weights():
        gate_row = iota((32, GROUP), 0)
        for n in range(4):
            for h in range(2):
                at = slice(2 * n + h, 2 * n + h + 1)
                mine = jnp.where(gate_row == 2 * t + h, G[n], 0.0)
                IG[at, :] = jnp.sum(mine, axis=0, keepdims=True) + offsets[n, 0, h : h + 1, :]
                mine = jnp.where(gate_row == 16 + 2 * t + h, G[n], 0.0)
                PRE[at, :] = jnp.sum(mine, axis=0, keepdims=True) + bias[h]
                LF[at, :] = offsets[n, 1, h : h + 1, :]

        wide_lane = iota((8, GROUP), 1)
        pre = PRE[...]
        soft = jnp.minimum(pre, 0.0) - jnp.log1p(jnp.exp(-jnp.abs(pre)))
        log_forget = soft + LF[...]
        suffix = log_forget
        step = 1
        while step < GROUP:
            suffix = suffix + jnp.where(wide_lane < GROUP - step, pltpu.roll(suffix, GROUP - step, 1), 0.0)
            step *= 2
        exclusive = jnp.where(wide_lane < GROUP - 1, pltpu.roll(suffix, GROUP - 1, 1), 0.0)
        local = IG[...] + exclusive
        LOC[...] = local
        total = suffix[:, 0:1]
        most = jnp.max(local, axis=1, keepdims=True)
        tail_part = jnp.where(lane - 64 == head_row, total, jnp.where(lane - 72 == head_row, most, 0.0))
        tail_part = jnp.broadcast_to(jnp.sum(tail_part, axis=0, keepdims=True), (8, 128))
        for half in range(2):
            part = local[:, half * 128 : (half + 1) * 128]
            for k in range(4):
                first = pltpu.roll(part, (128 - 32 * k) % 128, 1) if k else part
                second = pltpu.roll(pltpu.roll(part, 7, 0), (160 - 32 * k) % 128, 1) if k != 1 else pltpu.roll(part, 7, 0)
                row = jnp.where(lane < 32, first, jnp.where(lane < 64, second, tail_part))
                for n in range(4):
                    S[n * 8 + half * 4 + k] = row[2 * n : 2 * n + 1, :]
        R[pl.ds(s, 1)] = S[pl.ds(s, 1)]

        def send_rows(o, carry):
            peer = (s + o) % 32
            pltpu.make_async_remote_copy(
                src_ref=S.at[peer],
                dst_ref=R.at[s],
                send_sem=lws,
                recv_sem=lwr,
                device_id={"sp": peer},
                device_id_type=MESH,
            ).start()
            return carry

        lax.fori_loop(1, 32, send_rows, 0)

    def block_of(owner, i):
        at = ((owner - s + i + 32) % 8 + 8 * slot(i)) * BLOCK
        return T.at[pl.ds(pl.multiple_of(at, BLOCK), BLOCK)]

    def pass_on(owner, i, to, recv):
        block = block_of(owner, i)
        pltpu.make_async_remote_copy(
            src_ref=block,
            dst_ref=block,
            send_sem=xs,
            recv_sem=recv,
            device_id={"tp": to},
            device_id_type=MESH,
        ).start()

    half_block = BLOCK // 2

    def pass_half(owner, i, half, to):
        at = ((owner - s + i + 32) % 8 + 8 * slot(i)) * BLOCK + half * half_block
        part = T.at[pl.ds(pl.multiple_of(at, half_block), half_block)]
        pltpu.make_async_remote_copy(
            src_ref=part,
            dst_ref=part,
            send_sem=xs,
            recv_sem=xf.at[i, half],
            device_id={"tp": to},
            device_id_type=MESH,
        ).start()

    one_block = T.at[0:BLOCK]

    def stage_a(j):
        i = due_at(j)
        arrived(one_block, p1r.at[i])
        pass_on(t, i, right, xl.at[i])
        pass_on(t, i, left, xr.at[i])
        pass_on(t, i, mate, dr.at[i])

    def stage_b(j):
        i = due_at(j)
        arrived(one_block, xl.at[i])
        pass_half(left, i, 0, right)
        pass_on(left, i, mate, dr.at[i])
        arrived(one_block, xr.at[i])
        pass_half(right, i, 1, left)
        pass_on(right, i, mate, dr.at[i])

    def stage_c(j):
        i = due_at(j)
        arrived(T.at[0:half_block], xf.at[i, 0])
        arrived(T.at[0:half_block], xf.at[i, 1])
        pass_on(across, i, mate, dr.at[i])

    def write_out(i):
        at = pl.ds(pl.multiple_of(slot(i) * GROUP, GROUP), GROUP)
        return (
            pltpu.make_async_copy(OK.at[at], out_keys.at[at], loc.at[6]),
            pltpu.make_async_copy(OV.at[at], out_values.at[at], loc.at[7]),
        )

    def stage_n(j):
        i = due_at(j)
        arrived(T.at[0 : 4 * BLOCK], dr.at[i])
        start = pl.multiple_of(slot(i) * GROUP, GROUP)
        norm_group(T, start, N, j * GROUP, gain)

    def stage_d(j):
        i = due_at(j)
        start = pl.multiple_of(slot(i) * GROUP, GROUP)
        keys, values = project(N[j * GROUP : (j + 1) * GROUP, :])
        OK[pl.ds(start, GROUP), :] = keys
        OV[pl.ds(start, GROUP), :] = values
        for copy in write_out(i):
            copy.start()

    def column(row, first):
        return jnp.sum(jnp.where(lane - first == head_row, row, 0.0), axis=1, keepdims=True)

    def log_weights():
        arrived(R.at[0:31], lwr)
        received = R[:, 0, :]
        row = iota((32, 128), 0)
        lane32 = iota((32, 128), 1)
        suffix = received
        step = 1
        while step < 32:
            suffix = suffix + jnp.where(row < 32 - step, pltpu.roll(suffix, 32 - step, 0), 0.0)
            step *= 2
        exclusive = jnp.where(row < 31, pltpu.roll(suffix, 31, 0), 0.0)
        peaks = jnp.max(received + pltpu.roll(exclusive, 8, 1), axis=0, keepdims=True)
        PEAK[...] = jnp.broadcast_to(column(peaks, 72), (8, 128))
        mine = jnp.sum(jnp.where(row == s, exclusive, 0.0), axis=0, keepdims=True)
        LOC[...] += column(mine, 64)
        tails = [
            jnp.sum(jnp.where(lane32 == 64 + 2 * n_me + h, exclusive, 0.0), axis=1, keepdims=True)
            for h in range(2)
        ]
        L[...] = received + jnp.where(lane32 < 32, tails[0], tails[1])
        for h in range(2):
            wide = jnp.zeros((8, 128), F32)
            for k in range(4):
                rows = L[pl.ds(k, 8, stride=4), :]
                shift = (32 * k - 32 * h) % 128
                moved = pltpu.roll(rows, shift, 1) if shift else rows
                wide = jnp.where((lane >= 32 * k) & (lane < 32 * k + 32), moved, wide)
            for g in range(8):
                LW[h : h + 1, g * 128 : (g + 1) * 128] = wide[g : g + 1, :]
        out_weights[...] = LW[...]

        query = new_query[...].astype(F32)
        for n in range(4):
            Q8[2 * n : 2 * n + 1, :] = jnp.where(lane1 < 64, query[n : n + 1, :], 0.0)
            Q8[2 * n + 1 : 2 * n + 2, :] = jnp.where(lane1 < 64, 0.0, query[n : n + 1, :])
        NUM[...] = jnp.zeros_like(NUM)
        DEN[...] = jnp.zeros_like(DEN)

    def project(rows):
        both = jnp.dot(rows, W[...].reshape(D, 384), preferred_element_type=F32)
        return (both[:, 0:128] * 0.125).astype(BF16), both[:, 128:384].astype(BF16)

    def own_read(n):
        keys, values = project(X[n * GROUP : (n + 1) * GROUP, :])
        scores = lax.dot_general(Q8[...].astype(BF16), keys, NT, preferred_element_type=F32)
        terms = jnp.exp(LOC[...] - PEAK[:, 0:1]) * scores
        terms = jnp.where(iota((8, GROUP), 0) // 2 == n, terms, 0.0)
        DEN[...] += jnp.broadcast_to(jnp.sum(terms, axis=1, keepdims=True), (8, 128))
        NUM[...] += jnp.dot(terms.astype(BF16), values, preferred_element_type=F32)

    def share(buffer, slot_of, peers, send, recv):
        for to in peers:
            pltpu.make_async_remote_copy(
                src_ref=buffer.at[slot_of],
                dst_ref=buffer.at[slot_of],
                send_sem=send,
                recv_sem=recv,
                device_id={"sp": to},
                device_id_type=MESH,
            ).start()

    def sum_y():
        value = jnp.where(head_row % 2 == 0, NUM[:, 0:128], NUM[:, 128:256])
        E1[pl.ds(y, 1)] = jnp.concatenate([value, DEN[...]], axis=0).reshape(1, 16, 128)
        share(E1, y, [z * 4 + (y + o) % 4 for o in range(1, 4)], es.at[0], er.at[0])

    def sum_z():
        arrived(E1.at[0:3], er.at[0])
        E2[pl.ds(z, 1)] = ((E1[0] + E1[1]) + (E1[2] + E1[3])).reshape(1, 16, 128)
        share(E2, z, [((z + o) % 8) * 4 + y for o in range(1, 8)], es.at[1], er.at[1])

    def finish():
        arrived(E2.at[0:7], er.at[1])
        total = jnp.sum(E2[...], axis=0)
        numerator, denominator = total[0:8], total[8:16, 0:1]
        peak = PEAK[:, 0:1]
        gate = jnp.sum(
            jnp.where(iota((8, 32), 1) == 2 * t + iota((8, 32), 0) % 2, GN8[...], 0.0), axis=1, keepdims=True
        )
        own = jnp.sum(Q8[...] * (KN8[...] * 0.125).astype(BF16).astype(F32), axis=1, keepdims=True)
        top = jnp.maximum(peak, gate)
        old_part = jnp.exp(peak - top)
        new_part = jnp.exp(gate - top) * own
        value = old_part * numerator + new_part * VN8[...].astype(BF16).astype(F32)
        weight = old_part * denominator + new_part
        read = value / jnp.maximum(jnp.abs(weight), 1.0)
        for n in range(4):
            for h in range(2):
                A0[n : n + 1, h * 128 : (h + 1) * 128] = read[2 * n + h : 2 * n + h + 1, :]
        out_read[...] = A0[...].astype(BF16)

    lane1 = iota((1, 128), 1)

    def new_row_parts():
        total = jnp.zeros((4, 128), F32)
        for g in range(D // 128):
            v = new_rows[:, g * 128 : (g + 1) * 128].astype(F32)
            total = total + v * v
        inverse = lax.rsqrt(jnp.sum(total, axis=-1, keepdims=True) * (1.0 / D) + EPSILON)
        NN[...] = jnp.zeros_like(NN)
        for g in range(D // 128):
            at = slice(g * 128, (g + 1) * 128)
            NN[0:4, at] = new_rows[:, at].astype(F32) * inverse * gain[g : g + 1, :].astype(F32)
        fresh = NN[...].astype(BF16)
        both = jnp.dot(fresh, W[...].reshape(D, 384), preferred_element_type=F32)
        gates_new = lax.dot_general(fresh, GW[...], NT, preferred_element_type=F32)
        for n in range(4):
            for h in range(2):
                at = slice(2 * n + h, 2 * n + h + 1)
                KN8[at, :] = both[n : n + 1, 0:128]
                VN8[at, :] = both[n : n + 1, 128 * (h + 1) : 128 * (h + 2)]
                GN8[at, :] = gates_new[n : n + 1, :]

    for copy in small:
        copy.wait()
    for n in range(4):
        gates(n)
    local_weights()
    arrived(W.at[0, 0], wc)
    for o in range(1, 4):
        shard_to(far_z, half_z + (z + o) % 4, w2)
    arrived(W.at[0:3, 0], wh)
    y_send(half_z, y, up, 0)
    y_send(half_z, y, down, 1)
    start_leg(1)

    @pl.when(inner == 0)
    def _():
        start_leg(2)

    stage_a(0)
    stage_b(0)

    @pl.when(inner == 1)
    def _():
        start_leg(2)

    start_leg(3)
    arrived(W.at[0:4, 0], wy.at[0])
    y_send(half_z, down, up, 2)
    arrived(W.at[0:3, 0], w2)
    y_send(other_z, y, up, 3)
    y_send(other_z, y, down, 4)
    stage_a(1)
    stage_c(0)
    arrived(W.at[0:4, 0], wy.at[4])
    y_send(other_z, up, down, 5)
    stage_a(2)
    stage_b(1)
    stage_n(0)
    log_weights()
    stage_b(2)
    stage_a(3)
    stage_c(1)
    for which in (1, 2, 3, 5):
        arrived(W.at[0:4, 0], wy.at[which])
    own_read(0)
    stage_c(2)
    own_read(1)
    stage_b(3)
    own_read(2)
    own_read(3)
    sum_y()
    stage_c(3)
    stage_n(1)
    stage_d(0)
    stage_d(1)
    sum_z()
    new_row_parts()
    stage_n(2)
    stage_d(2)
    stage_n(3)
    stage_d(3)
    finish()
    arrived(OK, loc.at[6])
    arrived(OV, loc.at[7])

    arrived(R.at[0:31], lws)
    arrived(E1.at[0:3], es.at[0])
    arrived(E2.at[0:7], es.at[1])
    arrived(W.at[0:7, 0], ws1)
    arrived(W.at[0:6], ws2)
    arrived(T.at[0 : 28 * BLOCK], xs)

    def leg_done(i):
        dest, _, _, remote = first_leg(i)

        @pl.when(dest != s)
        def _():
            remote.wait_send()

    for i in range(4):
        leg_done(i)


def place(keys, values, weights, read, out_keys, out_values, out_weights, out_read, sems):
    copies = [
        pltpu.make_async_copy(keys, out_keys.at[0], sems.at[0]),
        pltpu.make_async_copy(values, out_values.at[0], sems.at[1]),
        pltpu.make_async_copy(weights, out_weights.at[0], sems.at[2]),
        pltpu.make_async_copy(read, out_read, sems.at[3]),
    ]
    for copy in copies:
        copy.start()
    for copy in copies:
        copy.wait()


def per_device(
    tokens,
    new_rows,
    new_query,
    norm_gain,
    key_weight,
    value_weight,
    input_weight,
    forget_weight,
    forget_bias,
    gate_offsets,
):
    any_space = pl.BlockSpec(memory_space=pl.ANY)
    vmem = pl.BlockSpec(memory_space=pltpu.VMEM)
    smem = pl.BlockSpec(memory_space=pltpu.SMEM)
    dma = pltpu.SemaphoreType.DMA
    keys, values, weights, read = pl.pallas_call(
        kernel,
        out_shape=(
            jax.ShapeDtypeStruct((ROWS, 128), BF16),
            jax.ShapeDtypeStruct((ROWS, 256), BF16),
            jax.ShapeDtypeStruct((2, ROWS), F32),
            jax.ShapeDtypeStruct((4, 256), BF16),
        ),
        in_specs=[any_space] * 8 + [smem, any_space],
        out_specs=(any_space, any_space, vmem, vmem),
        scratch_shapes=[
            pltpu.VMEM((4, D), BF16),
            pltpu.VMEM((4, 128), BF16),
            pltpu.VMEM((16, 128), BF16),
            pltpu.VMEM((4, 2, 2, GROUP), F32),
            pltpu.VMEM((ROWS, D), BF16),
            pltpu.VMEM((ROWS, D), BF16),
            pltpu.VMEM((ROWS, D), BF16),
            pltpu.VMEM((8, 4, 64, 384), BF16),
            pltpu.VMEM((ROWS, 128), BF16),
            pltpu.VMEM((ROWS, 256), BF16),
            pltpu.VMEM((4, 32, GROUP), F32),
            pltpu.VMEM((32, D), BF16),
            pltpu.VMEM((8, D), F32),
            pltpu.VMEM((8, GROUP), F32),
            pltpu.VMEM((8, GROUP), F32),
            pltpu.VMEM((8, GROUP), F32),
            pltpu.VMEM((8, GROUP), F32),
            pltpu.VMEM((32, 1, 128), F32),
            pltpu.VMEM((32, 1, 128), F32),
            pltpu.VMEM((32, 128), F32),
            pltpu.VMEM((2, ROWS), F32),
            pltpu.VMEM((8, 128), F32),
            pltpu.VMEM((8, 128), F32),
            pltpu.VMEM((8, 256), F32),
            pltpu.VMEM((8, 128), F32),
            pltpu.VMEM((8, 128), F32),
            pltpu.VMEM((8, 128), F32),
            pltpu.VMEM((8, 32), F32),
            pltpu.VMEM((4, 16, 128), F32),
            pltpu.VMEM((8, 16, 128), F32),
            pltpu.VMEM((4, 256), F32),
            dma((4,)),
            dma((4,)),
            dma((4,)),
            dma((4,)),
            dma((4, 2)),
            dma((4,)),
            dma,
            dma,
            dma,
            dma,
            dma,
            dma,
            dma((6,)),
            dma,
            dma,
            dma((2,)),
            dma((2,)),
            dma((14,)),
        ],
        compiler_params=pltpu.CompilerParams(collective_id=0, has_side_effects=True),
    )(
        tokens.reshape(ROWS, D),
        new_rows,
        new_query,
        norm_gain.reshape(16, 128),
        key_weight,
        value_weight,
        input_weight.T,
        forget_weight.T,
        forget_bias,
        jnp.transpose(gate_offsets, (0, 2, 3, 1)),
    )
    return pl.pallas_call(
        place,
        out_shape=(
            jax.ShapeDtypeStruct((1, ROWS, 128), BF16),
            jax.ShapeDtypeStruct((1, ROWS, 256), BF16),
            jax.ShapeDtypeStruct((1, 2, ROWS), F32),
            jax.ShapeDtypeStruct((4, 256), BF16),
        ),
        in_specs=[vmem] * 4,
        out_specs=[any_space] * 4,
        scratch_shapes=[dma((4,))],
    )(keys, values, weights, read)


def solution(mesh):
    return jax.shard_map(
        per_device,
        mesh=mesh,
        in_specs=(
            P("gr", "sp", None),
            P("gr", None),
            P("gr", "tp"),
            P(),
            P("sp", "tp"),
            P("sp", "tp"),
            P(),
            P(),
            P("tp"),
            P("gr", "sp", None, "tp"),
        ),
        out_specs=(
            P(("gr", "sp"), None, "tp"),
            P(("gr", "sp"), None, "tp"),
            P(("gr", "sp"), "tp", None),
            P("gr", "tp"),
        ),
        check_vma=False,
    )
```

time: 79 us -> 77.3 us (0.978)
  the two profiles are of different devices: /device:TPU:1 before, /device:TPU:8 now
where the time goes in v3:
time: 77.3 us; the launch traced here: 77.1 us
  Pallas kernels  76.4 us (99%)
    pallas_call x1, Pallas kernels, per_device(): pl.pallas_call(kernel, out_shape=(jax.ShapeDtypeStruct((ROWS, 128), BF16)...  74.4 us
    pallas_call x1, Pallas kernels, per_device(): pl.pallas_call(place, out_shape=(jax.ShapeDtypeStruct((1, ROWS, 128), BF1...  2.03 us

profile of v3, /device:TPU:8, one launch (start us, length us, event | category | flops | bytes accessed | tf_op | source)
XLA Modules:
  0.0 77.1 jit_solution(7481654462508552834)
XLA Ops:
  0.6 74.4 %shard_map.129 = (bf16[1024,128]{1,0:T(8,128)(2,1)}, bf16[1024,256]{1,0:T(8,128)(2,1)}, f32[2,1024]{1,0:T(2,128)}, bf16[4,256]{1,0:T(4,128)(2,1)}) custom-call(bf16[1024,2048]{1,0:T(8,128)(2,1)} %bitcast.5, bf16[4,2048]{1,0:T(4,128)(2,1)} %new_rows_in.1, bf16[4,128]{1,0:T(4,128)(2,1)} %new_query_in.1, bf16[16,128]{1,0:T(8,128)(2,1)} %bitcast.9, ...), custom_call_target="tpu_custom_call" | custom-call | tf_op jit(solution)/shard_map/pallas_call | solution.py:607
  75.1 2.0 %shard_map.130 = (bf16[1,1024,128]{2,1,0:T(8,128)(2,1)}, bf16[1,1024,256]{2,1,0:T(8,128)(2,1)}, f32[1,2,1024]{2,1,0:T(2,128)}, bf16[4,256]{1,0:T(4,128)(2,1)}) custom-call(bf16[1024,128]{1,0:T(8,128)(2,1)} %get-tuple-element.8.keys, bf16[1024,256]{1,0:T(8,128)(2,1)} %get-tuple-element.9.values, f32[2,1024]{1,0:T(2,128)} %get-tuple-element.10.weights, ...), custom_call_target="tpu_custom_call" | custom-call | tf_op jit(solution)/shard_map/pallas_call | solution.py:681

commit v4 on v3

--- a/solution.py
+++ b/solution.py
@@ -221,11 +221,11 @@
         def _():
             pltpu.make_async_copy(src, dst, p1r.at[i]).start()
 
+    start_leg(0)
     shard_to(z, far_z, wc)
     for o in range(1, 4):
         shard_to(z, half_z + (z + o) % 4, wh)
 
-    start_leg(0)
 
     def y_send(rows, column, to_y, which):
         pltpu.make_async_remote_copy(
@@ -510,19 +510,19 @@
     def _():
         start_leg(2)
 
-    stage_a(0)
-    stage_b(0)
+    arrived(W.at[0:4, 0], wy.at[0])
+    y_send(half_z, down, up, 2)
 
     @pl.when(inner == 1)
     def _():
         start_leg(2)
 
     start_leg(3)
-    arrived(W.at[0:4, 0], wy.at[0])
-    y_send(half_z, down, up, 2)
+    stage_a(0)
     arrived(W.at[0:3, 0], w2)
     y_send(other_z, y, up, 3)
     y_send(other_z, y, down, 4)
+    stage_b(0)
     stage_a(1)
     stage_c(0)
     arrived(W.at[0:4, 0], wy.at[4])
@@ -533,21 +533,21 @@
     log_weights()
     stage_b(2)
     stage_a(3)
-    stage_c(1)
     for which in (1, 2, 3, 5):
         arrived(W.at[0:4, 0], wy.at[which])
     own_read(0)
+    own_read(1)
+    stage_c(1)
     stage_c(2)
-    own_read(1)
-    stage_b(3)
     own_read(2)
     own_read(3)
     sum_y()
-    stage_c(3)
+    stage_b(3)
     stage_n(1)
     stage_d(0)
+    sum_z()
+    stage_c(3)
     stage_d(1)
-    sum_z()
     new_row_parts()
     stage_n(2)
     stage_d(2)

time: 77.3 us -> 74.9 us (0.969)
  the two profiles are of different devices: /device:TPU:8 before, /device:TPU:1 now
where the time goes in v4:
time: 74.9 us; the launch traced here: 74.5 us
  Pallas kernels  73.8 us (99%)
    pallas_call x1, Pallas kernels, per_device(): pl.pallas_call(kernel, out_shape=(jax.ShapeDtypeStruct((ROWS, 128), BF16)...  71.8 us
    pallas_call x1, Pallas kernels, per_device(): pl.pallas_call(place, out_shape=(jax.ShapeDtypeStruct((1, ROWS, 128), BF1...  2.03 us

profile of v4, /device:TPU:1, one launch (start us, length us, event | category | flops | bytes accessed | tf_op | source)
XLA Modules:
  0.0 74.5 jit_solution(320537183178836)
XLA Ops:
  0.6 71.8 %shard_map.129 = (bf16[1024,128]{1,0:T(8,128)(2,1)}, bf16[1024,256]{1,0:T(8,128)(2,1)}, f32[2,1024]{1,0:T(2,128)}, bf16[4,256]{1,0:T(4,128)(2,1)}) custom-call(bf16[1024,2048]{1,0:T(8,128)(2,1)} %bitcast.5, bf16[4,2048]{1,0:T(4,128)(2,1)} %new_rows_in.1, bf16[4,128]{1,0:T(4,128)(2,1)} %new_query_in.1, bf16[16,128]{1,0:T(8,128)(2,1)} %bitcast.9, ...), custom_call_target="tpu_custom_call" | custom-call | tf_op jit(solution)/shard_map/pallas_call | solution.py:607
  72.4 2.0 %shard_map.130 = (bf16[1,1024,128]{2,1,0:T(8,128)(2,1)}, bf16[1,1024,256]{2,1,0:T(8,128)(2,1)}, f32[1,2,1024]{2,1,0:T(2,128)}, bf16[4,256]{1,0:T(4,128)(2,1)}) custom-call(bf16[1024,128]{1,0:T(8,128)(2,1)} %get-tuple-element.8.keys, bf16[1024,256]{1,0:T(8,128)(2,1)} %get-tuple-element.9.values, f32[2,1024]{1,0:T(2,128)} %get-tuple-element.10.weights, ...), custom_call_target="tpu_custom_call" | custom-call | tf_op jit(solution)/shard_map/pallas_call | solution.py:681

commit v5 on v4

--- a/solution.py
+++ b/solution.py
@@ -187,10 +187,10 @@
     inner = (k_me // 2 + k_me % 2) % 2
 
     def sent_at(j):
-        return inner * (0, 1, 2, 3)[j] + (1 - inner) * (0, 3, 2, 1)[j]
+        return inner * (0, 1, 2, 3)[j] + (1 - inner) * ((1 - c) * (0, 3, 2, 1)[j] + c * (0, 2, 3, 1)[j])
 
     def due_at(j):
-        return inner * (0, 2, 1, 3)[j] + (1 - inner) * (0, 1, 3, 2)[j]
+        return inner * (0, 2, 1, 3)[j] + (1 - inner) * ((1 - c) * (0, 3, 1, 2)[j] + c * (0, 1, 3, 2)[j])
 
     def slot(i):
         return xor2(k_me, i)
@@ -319,40 +319,45 @@
 
     half_block = BLOCK // 2
 
-    def pass_half(owner, i, half, to):
+    def pass_half(owner, i, half, to, recv):
         at = ((owner - s + i + 32) % 8 + 8 * slot(i)) * BLOCK + half * half_block
         part = T.at[pl.ds(pl.multiple_of(at, half_block), half_block)]
         pltpu.make_async_remote_copy(
             src_ref=part,
             dst_ref=part,
             send_sem=xs,
-            recv_sem=xf.at[i, half],
+            recv_sem=recv,
             device_id={"tp": to},
             device_id_type=MESH,
         ).start()
 
     one_block = T.at[0:BLOCK]
 
+    half_rows = T.at[0:half_block]
+
     def stage_a(j):
         i = due_at(j)
         arrived(one_block, p1r.at[i])
-        pass_on(t, i, right, xl.at[i])
-        pass_on(t, i, left, xr.at[i])
+        for half in range(2):
+            pass_half(t, i, half, right, xl.at[i, half])
+            pass_half(t, i, 1 - half, left, xr.at[i, 1 - half])
         pass_on(t, i, mate, dr.at[i])
 
     def stage_b(j):
         i = due_at(j)
-        arrived(one_block, xl.at[i])
-        pass_half(left, i, 0, right)
+        arrived(half_rows, xl.at[i, 0])
+        pass_half(left, i, 0, right, xf.at[i, 0])
+        arrived(half_rows, xr.at[i, 1])
+        pass_half(right, i, 1, left, xf.at[i, 1])
+        arrived(half_rows, xl.at[i, 1])
         pass_on(left, i, mate, dr.at[i])
-        arrived(one_block, xr.at[i])
-        pass_half(right, i, 1, left)
+        arrived(half_rows, xr.at[i, 0])
         pass_on(right, i, mate, dr.at[i])
 
     def stage_c(j):
         i = due_at(j)
-        arrived(T.at[0:half_block], xf.at[i, 0])
-        arrived(T.at[0:half_block], xf.at[i, 1])
+        arrived(half_rows, xf.at[i, 0])
+        arrived(half_rows, xf.at[i, 1])
         pass_on(across, i, mate, dr.at[i])
 
     def write_out(i):
@@ -368,14 +373,15 @@
         start = pl.multiple_of(slot(i) * GROUP, GROUP)
         norm_group(T, start, N, j * GROUP, gain)
 
-    def stage_d(j):
-        i = due_at(j)
-        start = pl.multiple_of(slot(i) * GROUP, GROUP)
-        keys, values = project(N[j * GROUP : (j + 1) * GROUP, :])
-        OK[pl.ds(start, GROUP), :] = keys
-        OV[pl.ds(start, GROUP), :] = values
-        for copy in write_out(i):
-            copy.start()
+    def stage_d(j, groups=1):
+        keys, values = project(N[j * GROUP : (j + groups) * GROUP, :])
+        for g in range(groups):
+            i = due_at(j + g)
+            start = pl.multiple_of(slot(i) * GROUP, GROUP)
+            OK[pl.ds(start, GROUP), :] = keys[g * GROUP : (g + 1) * GROUP]
+            OV[pl.ds(start, GROUP), :] = values[g * GROUP : (g + 1) * GROUP]
+            for copy in write_out(i):
+                copy.start()
 
     def column(row, first):
         return jnp.sum(jnp.where(lane - first == head_row, row, 0.0), axis=1, keepdims=True)
@@ -423,10 +429,12 @@
         return (both[:, 0:128] * 0.125).astype(BF16), both[:, 128:384].astype(BF16)
 
     def own_read(n):
-        keys, values = project(X[n * GROUP : (n + 1) * GROUP, :])
+        keys, values = project(X[n * GROUP : (n + 2) * GROUP, :])
         scores = lax.dot_general(Q8[...].astype(BF16), keys, NT, preferred_element_type=F32)
-        terms = jnp.exp(LOC[...] - PEAK[:, 0:1]) * scores
-        terms = jnp.where(iota((8, GROUP), 0) // 2 == n, terms, 0.0)
+        weight = jnp.exp(LOC[...] - PEAK[:, 0:1])
+        terms = jnp.concatenate([weight, weight], axis=1) * scores
+        prompt = n + iota((8, 2 * GROUP), 1) // GROUP
+        terms = jnp.where(iota((8, 2 * GROUP), 0) // 2 == prompt, terms, 0.0)
         DEN[...] += jnp.broadcast_to(jnp.sum(terms, axis=1, keepdims=True), (8, 128))
         NUM[...] += jnp.dot(terms.astype(BF16), values, preferred_element_type=F32)
 
@@ -536,20 +544,17 @@
     for which in (1, 2, 3, 5):
         arrived(W.at[0:4, 0], wy.at[which])
     own_read(0)
-    own_read(1)
     stage_c(1)
     stage_c(2)
     own_read(2)
-    own_read(3)
     sum_y()
     stage_b(3)
     stage_n(1)
-    stage_d(0)
+    stage_d(0, 2)
     sum_z()
     stage_c(3)
-    stage_d(1)
+    stage_n(2)
     new_row_parts()
-    stage_n(2)
     stage_d(2)
     stage_n(3)
     stage_d(3)
@@ -648,8 +653,8 @@
             pltpu.VMEM((4, 256), F32),
             dma((4,)),
             dma((4,)),
-            dma((4,)),
-            dma((4,)),
+            dma((4, 2)),
+            dma((4, 2)),
             dma((4, 2)),
             dma((4,)),
             dma,

time: 74.9 us -> 71 us (0.948)
  Pallas kernels: 73.8 us -> 70.2 us
    pallas_call x1, Pallas kernels: 71.8 us -> 68.2 us  [per_device(): pl.pallas_call(kernel, out_shape=(jax.ShapeDtypeStruct((ROWS, 128), BF16)...]
where the time goes in v5:
time: 71 us; the launch traced here: 70.8 us
  Pallas kernels  70.2 us (99%)
    pallas_call x1, Pallas kernels, per_device(): pl.pallas_call(kernel, out_shape=(jax.ShapeDtypeStruct((ROWS, 128), BF16)...  68.2 us
    pallas_call x1, Pallas kernels, per_device(): pl.pallas_call(place, out_shape=(jax.ShapeDtypeStruct((1, ROWS, 128), BF1...  2.03 us

profile of v5, /device:TPU:1, one launch (start us, length us, event | category | flops | bytes accessed | tf_op | source)
XLA Modules:
  0.0 70.8 jit_solution(14119559590843063317)
XLA Ops:
  0.6 68.2 %shard_map.129 = (bf16[1024,128]{1,0:T(8,128)(2,1)}, bf16[1024,256]{1,0:T(8,128)(2,1)}, f32[2,1024]{1,0:T(2,128)}, bf16[4,256]{1,0:T(4,128)(2,1)}) custom-call(bf16[1024,2048]{1,0:T(8,128)(2,1)} %bitcast.5, bf16[4,2048]{1,0:T(4,128)(2,1)} %new_rows_in.1, bf16[4,128]{1,0:T(4,128)(2,1)} %new_query_in.1, bf16[16,128]{1,0:T(8,128)(2,1)} %bitcast.9, ...), custom_call_target="tpu_custom_call" | custom-call | tf_op jit(solution)/shard_map/pallas_call | solution.py:612
  68.8 2.0 %shard_map.130 = (bf16[1,1024,128]{2,1,0:T(8,128)(2,1)}, bf16[1,1024,256]{2,1,0:T(8,128)(2,1)}, f32[1,2,1024]{2,1,0:T(2,128)}, bf16[4,256]{1,0:T(4,128)(2,1)}) custom-call(bf16[1024,128]{1,0:T(8,128)(2,1)} %get-tuple-element.8.keys, bf16[1024,256]{1,0:T(8,128)(2,1)} %get-tuple-element.9.values, f32[2,1024]{1,0:T(2,128)} %get-tuple-element.10.weights, ...), custom_call_target="tpu_custom_call" | custom-call | tf_op jit(solution)/shard_map/pallas_call | solution.py:686

commit v6 on v5

--- a/solution.py
+++ b/solution.py
@@ -509,15 +509,15 @@
     arrived(W.at[0, 0], wc)
     for o in range(1, 4):
         shard_to(far_z, half_z + (z + o) % 4, w2)
+    start_leg(1)
+
+    @pl.when(inner == 0)
+    def _():
+        start_leg(2)
+
     arrived(W.at[0:3, 0], wh)
     y_send(half_z, y, up, 0)
     y_send(half_z, y, down, 1)
-    start_leg(1)
-
-    @pl.when(inner == 0)
-    def _():
-        start_leg(2)
-
     arrived(W.at[0:4, 0], wy.at[0])
     y_send(half_z, down, up, 2)
 
@@ -525,11 +525,19 @@
     def _():
         start_leg(2)
 
-    start_leg(3)
+    @pl.when(inner == 0)
+    def _():
+        start_leg(3)
+
     stage_a(0)
     arrived(W.at[0:3, 0], w2)
     y_send(other_z, y, up, 3)
     y_send(other_z, y, down, 4)
+
+    @pl.when(inner == 1)
+    def _():
+        start_leg(3)
+
     stage_b(0)
     stage_a(1)
     stage_c(0)
@@ -544,20 +552,20 @@
     for which in (1, 2, 3, 5):
         arrived(W.at[0:4, 0], wy.at[which])
     own_read(0)
-    stage_c(1)
-    stage_c(2)
     own_read(2)
     sum_y()
+    stage_c(1)
     stage_b(3)
+    stage_c(2)
     stage_n(1)
-    stage_d(0, 2)
     sum_z()
     stage_c(3)
+    stage_d(0, 2)
     stage_n(2)
-    new_row_parts()
     stage_d(2)
     stage_n(3)
     stage_d(3)
+    new_row_parts()
     finish()
     arrived(OK, loc.at[6])
     arrived(OV, loc.at[7])

time: 71 us -> 71 us (level)
  no operation moved by 1% of the time
where the time goes in v6:
time: 71 us; the launch traced here: 70.8 us
  Pallas kernels  70.2 us (99%)
    pallas_call x1, Pallas kernels, per_device(): pl.pallas_call(kernel, out_shape=(jax.ShapeDtypeStruct((ROWS, 128), BF16)...  68.2 us
    pallas_call x1, Pallas kernels, per_device(): pl.pallas_call(place, out_shape=(jax.ShapeDtypeStruct((1, ROWS, 128), BF1...  2.03 us

profile of v6, /device:TPU:1, one launch (start us, length us, event | category | flops | bytes accessed | tf_op | source)
XLA Modules:
  0.0 70.8 jit_solution(14270518032109776193)
XLA Ops:
  0.6 68.2 %shard_map.129 = (bf16[1024,128]{1,0:T(8,128)(2,1)}, bf16[1024,256]{1,0:T(8,128)(2,1)}, f32[2,1024]{1,0:T(2,128)}, bf16[4,256]{1,0:T(4,128)(2,1)}) custom-call(bf16[1024,2048]{1,0:T(8,128)(2,1)} %bitcast.5, bf16[4,2048]{1,0:T(4,128)(2,1)} %new_rows_in.1, bf16[4,128]{1,0:T(4,128)(2,1)} %new_query_in.1, bf16[16,128]{1,0:T(8,128)(2,1)} %bitcast.9, ...), custom_call_target="tpu_custom_call" | custom-call | tf_op jit(solution)/shard_map/pallas_call | solution.py:620
  68.8 2.0 %shard_map.130 = (bf16[1,1024,128]{2,1,0:T(8,128)(2,1)}, bf16[1,1024,256]{2,1,0:T(8,128)(2,1)}, f32[1,2,1024]{2,1,0:T(2,128)}, bf16[4,256]{1,0:T(4,128)(2,1)}) custom-call(bf16[1024,128]{1,0:T(8,128)(2,1)} %get-tuple-element.8.keys, bf16[1024,256]{1,0:T(8,128)(2,1)} %get-tuple-element.9.values, f32[2,1024]{1,0:T(2,128)} %get-tuple-element.10.weights, ...), custom_call_target="tpu_custom_call" | custom-call | tf_op jit(solution)/shard_map/pallas_call | solution.py:694

commit v7 on v5

--- a/solution.py
+++ b/solution.py
@@ -509,15 +509,15 @@
     arrived(W.at[0, 0], wc)
     for o in range(1, 4):
         shard_to(far_z, half_z + (z + o) % 4, w2)
+    start_leg(1)
+
+    @pl.when(inner == 0)
+    def _():
+        start_leg(2)
+
     arrived(W.at[0:3, 0], wh)
     y_send(half_z, y, up, 0)
     y_send(half_z, y, down, 1)
-    start_leg(1)
-
-    @pl.when(inner == 0)
-    def _():
-        start_leg(2)
-
     arrived(W.at[0:4, 0], wy.at[0])
     y_send(half_z, down, up, 2)
 
@@ -580,17 +580,24 @@
         leg_done(i)
 
 
-def place(keys, values, weights, read, out_keys, out_values, out_weights, out_read, sems):
-    copies = [
-        pltpu.make_async_copy(keys, out_keys.at[0], sems.at[0]),
-        pltpu.make_async_copy(values, out_values.at[0], sems.at[1]),
-        pltpu.make_async_copy(weights, out_weights.at[0], sems.at[2]),
-        pltpu.make_async_copy(read, out_read, sems.at[3]),
-    ]
-    for copy in copies:
-        copy.start()
-    for copy in copies:
-        copy.wait()
+def place(keys, values, weights, read, out_keys, out_values, out_weights, out_read, k, v, w, r, came, left):
+    legs = []
+    for at, (src, held, dst) in enumerate(
+        (
+            (values, v, out_values.at[0]),
+            (keys, k, out_keys.at[0]),
+            (weights, w, out_weights.at[0]),
+            (read, r, out_read),
+        )
+    ):
+        arrive = pltpu.make_async_copy(src, held, came.at[at])
+        arrive.start()
+        legs.append((arrive, pltpu.make_async_copy(held, dst, left.at[at])))
+    for arrive, leave in reversed(legs):
+        arrive.wait()
+        leave.start()
+    for _, leave in legs:
+        leave.wait()
 
 
 def per_device(
@@ -691,9 +698,16 @@
             jax.ShapeDtypeStruct((1, 2, ROWS), F32),
             jax.ShapeDtypeStruct((4, 256), BF16),
         ),
-        in_specs=[vmem] * 4,
+        in_specs=[any_space] * 4,
         out_specs=[any_space] * 4,
-        scratch_shapes=[dma((4,))],
+        scratch_shapes=[
+            pltpu.VMEM((ROWS, 128), BF16),
+            pltpu.VMEM((ROWS, 256), BF16),
+            pltpu.VMEM((2, ROWS), F32),
+            pltpu.VMEM((4, 256), BF16),
+            dma((4,)),
+            dma((4,)),
+        ],
     )(keys, values, weights, read)
 
 

time: 71 us -> 71.6 us (level)
  no operation moved by 1% of the time
where the time goes in v7:
time: 71.6 us; the launch traced here: 71.4 us
  Pallas kernels  70.8 us (99%)
    pallas_call x1, Pallas kernels, per_device(): pl.pallas_call(kernel, out_shape=(jax.ShapeDtypeStruct((ROWS, 128), BF16)...  68.7 us
    pallas_call x1, Pallas kernels, per_device(): pl.pallas_call(place, out_shape=(jax.ShapeDtypeStruct((1, ROWS, 128), BF1...  2.06 us

profile of v7, /device:TPU:1, one launch (start us, length us, event | category | flops | bytes accessed | tf_op | source)
XLA Modules:
  0.0 71.4 jit_solution(2494483159014837763)
XLA Ops:
  0.6 68.7 %shard_map.129 = (bf16[1024,128]{1,0:T(8,128)(2,1)}, bf16[1024,256]{1,0:T(8,128)(2,1)}, f32[2,1024]{1,0:T(2,128)}, bf16[4,256]{1,0:T(4,128)(2,1)}) custom-call(bf16[1024,2048]{1,0:T(8,128)(2,1)} %bitcast.5, bf16[4,2048]{1,0:T(4,128)(2,1)} %new_rows_in.1, bf16[4,128]{1,0:T(4,128)(2,1)} %new_query_in.1, bf16[16,128]{1,0:T(8,128)(2,1)} %bitcast.9, ...), custom_call_target="tpu_custom_call" | custom-call | tf_op jit(solution)/shard_map/pallas_call | solution.py:619
  69.4 2.1 %shard_map.130 = (bf16[1,1024,128]{2,1,0:T(8,128)(2,1)}, bf16[1,1024,256]{2,1,0:T(8,128)(2,1)}, f32[1,2,1024]{2,1,0:T(2,128)}, bf16[4,256]{1,0:T(4,128)(2,1)}) custom-call(bf16[1024,128]{1,0:T(8,128)(2,1)} %get-tuple-element.8.keys, bf16[1024,256]{1,0:T(8,128)(2,1)} %get-tuple-element.9.values, f32[2,1024]{1,0:T(2,128)} %get-tuple-element.10.weights, ...), custom_call_target="tpu_custom_call" | custom-call | tf_op jit(solution)/shard_map/pallas_call | solution.py:693

commit v8 on v5

--- a/solution.py
+++ b/solution.py
@@ -132,8 +132,10 @@
 
     barrier = pltpu.get_barrier_semaphore()
 
+    way = 2 * (z // 4) - 1
+
     def greet(o, carry):
-        pl.semaphore_signal(barrier, inc=1, device_id={"sp": (s + o) % 32}, device_id_type=MESH)
+        pl.semaphore_signal(barrier, inc=1, device_id={"sp": (s + way * o + 32) % 32}, device_id_type=MESH)
         return carry
 
     lax.fori_loop(1, 32, greet, 0)

time: 71 us -> 71 us (level)
  no operation moved by 1% of the time
where the time goes in v8:
time: 71 us; the launch traced here: 70.8 us
  Pallas kernels  70.1 us (99%)
    pallas_call x1, Pallas kernels, per_device(): pl.pallas_call(kernel, out_shape=(jax.ShapeDtypeStruct((ROWS, 128), BF16)...  68.1 us
    pallas_call x1, Pallas kernels, per_device(): pl.pallas_call(place, out_shape=(jax.ShapeDtypeStruct((1, ROWS, 128), BF1...  2.03 us

profile of v8, /device:TPU:1, one launch (start us, length us, event | category | flops | bytes accessed | tf_op | source)
XLA Modules:
  0.0 70.8 jit_solution(1564802051741431394)
XLA Ops:
  0.6 68.1 %shard_map.129 = (bf16[1024,128]{1,0:T(8,128)(2,1)}, bf16[1024,256]{1,0:T(8,128)(2,1)}, f32[2,1024]{1,0:T(2,128)}, bf16[4,256]{1,0:T(4,128)(2,1)}) custom-call(bf16[1024,2048]{1,0:T(8,128)(2,1)} %bitcast.5, bf16[4,2048]{1,0:T(4,128)(2,1)} %new_rows_in.1, bf16[4,128]{1,0:T(4,128)(2,1)} %new_query_in.1, bf16[16,128]{1,0:T(8,128)(2,1)} %bitcast.9, ...), custom_call_target="tpu_custom_call" | custom-call | tf_op jit(solution)/shard_map/pallas_call | solution.py:614
  68.7 2.0 %shard_map.130 = (bf16[1,1024,128]{2,1,0:T(8,128)(2,1)}, bf16[1,1024,256]{2,1,0:T(8,128)(2,1)}, f32[1,2,1024]{2,1,0:T(2,128)}, bf16[4,256]{1,0:T(4,128)(2,1)}) custom-call(bf16[1024,128]{1,0:T(8,128)(2,1)} %get-tuple-element.8.keys, bf16[1024,256]{1,0:T(8,128)(2,1)} %get-tuple-element.9.values, f32[2,1024]{1,0:T(2,128)} %get-tuple-element.10.weights, ...), custom_call_target="tpu_custom_call" | custom-call | tf_op jit(solution)/shard_map/pallas_call | solution.py:688
